TPU v7x, 32 devices: a whole 2x2x4 slice. The times are simulated.
32 devices in a mesh: ep: 4 (over y, x), tp: 8 (over z, core).
Axes of the slice: x: 2, y: 2, z: 4, core: 2. Of those that a mesh axis runs over, the one named last changes fastest.
Arguments:
- mixer_input_channels: bfloat16 [8192, 2048], P('ep', 'tp'), may hold values from -6 to 6
- output_gate_logits: bfloat16 [8192, 2048], P('ep', 'tp'), may hold values from -6 to 6
- head_group_input_map: bfloat16 [8192, 256], P('ep'), may hold values from -6 to 6
- head_group_output_map: bfloat16 [8192, 256], P('ep'), may hold values from -6 to 6
- input_channel_taps: bfloat16 [4, 2048], P(None, 'tp'), may hold values from -3 to 3
- input_map_taps: bfloat16 [4, 256], replicated, may hold values from -3 to 3
- output_map_taps: bfloat16 [4, 256], replicated, may hold values from -3 to 3
- step_logits: float32 [32, 8192], P('tp', 'ep'), may hold values from -5 to 5
- head_log_rate: float32 [32], P('tp'), may hold values from -20 to -2
- extra_log_decay: float32 [32, 8192], P('tp', 'ep'), may hold values from -1 to 0
- head_direct_scale: float32 [32], P('tp'), may hold values from 1 to 6
- gated_norm_scale: bfloat16 [2048], P('tp'), may hold values from 0.099609375 to 1.8984375
- mixer_output_weight: bfloat16 [2048, 2048], P('tp'), may hold values from -0.125 to 0.125
- second_batch_tokens: bfloat16 [1024, 2048], P('ep'), may hold values from -6 to 6
- pre_expert_norm_scale: bfloat16 [2048], replicated, may hold values from 0.099609375 to 1.8984375
- group_router_columns: bfloat16 [2048, 1], replicated
- expert_router_columns: bfloat16 [2048, 4], replicated
- routes: int32 [1024, 2], P('ep'), may hold values from 0 to 3, all different within a row; in each aligned block of 256 rows (0 to 255, 256 to 511, ...) at most 256 rows name the same one
- expert_gate_weight: bfloat16 [4, 2048, 4096], P('ep', None, 'tp'), may hold values from -0.125 to 0.125
- expert_up_weight: bfloat16 [4, 2048, 4096], P('ep', None, 'tp'), may hold values from -0.125 to 0.125
- expert_down_weight: bfloat16 [4, 4096, 2048], P('ep', 'tp'), may hold values from -0.125 to 0.125
Outputs:
- mixer_out: bfloat16 [8192, 2048], P(('ep', 'tp'))
- experts_out: bfloat16 [1024, 2048], P('ep', 'tp')
Inputs may be any that keep to these rules, and one draw needn't show every extreme that they name: `routes`: in each aligned block of 256 rows no expert is named more than 256 times, some expert exactly 256 times in some block; a row's two experts differ.
All inputs are finite; a program needn't handle non-finite values.
Results may differ from a plain program's by a relative error of at most 0.019.
Values may be sent and summed in bfloat16 or wider, within the bound.
A program may use at most 128 MiB of HBM per device.

v0:
```python
import jax
import jax.numpy as jnp
from jax import lax
from jax.sharding import PartitionSpec as P

HEADS = 32
STATE = 64
GROUPS = 4
BLOCK = 128
CORES = 2


eps = 1e-06
exact_prec = lax.Precision.DEFAULT


def from_behind(value, axis, steps):
    count = lax.axis_size(axis)
    first, last = (max(0, -steps), min(count, count - steps))
    return lax.ppermute(value, axis, [(source, source + steps) for source in range(first, last)])


def carried_in(state, decay, axis):
    rows = jnp.broadcast_to(decay[:, None, None], (state.shape[0], 8, state.shape[2]))
    packed = jnp.concatenate([state, rows], axis=1).astype(jnp.bfloat16)
    behind = [from_behind(packed, axis, step) for step in range(1, lax.axis_size(axis))]
    total = jnp.zeros_like(state)
    for one in reversed(behind):
        one = one.astype(jnp.float32)
        total = total * one[:, -1:, :1] + one[:, :-8]
    return total


def ring_shift(value, axis, steps):
    count = lax.axis_size(axis)
    return lax.ppermute(value, axis, [(s, (s + steps) % count) for s in range(count)])


def conv_with_rows(joined, before, taps):
    length = joined.shape[0]
    padded = jnp.concatenate([before, joined], axis=0).astype(jnp.float32)
    total = jnp.zeros(joined.shape, jnp.float32)
    for j in range(taps.shape[0]):
        total = total + taps[j].astype(jnp.float32) * padded[j : j + length]
    return jax.nn.silu(total).astype(jnp.bfloat16)


def route_weights(group_logits, expert_logits, routes):
    n_groups = group_logits.shape[1]
    n_experts = expert_logits.shape[1]
    per_group = n_experts // n_groups
    group_lp = jax.nn.log_softmax(group_logits, axis=-1)
    inner_lp = jax.nn.log_softmax(expert_logits.reshape(-1, n_groups, per_group), axis=-1).reshape(
        -1, n_experts
    )
    total = jnp.repeat(group_lp, per_group, axis=1) + inner_lp
    pick = routes[:, :, None] == jnp.arange(n_experts, dtype=jnp.int32)[None, None, :]
    chosen = jnp.sum(jnp.where(pick, total[:, None, :], 0.0), axis=-1)
    share = jax.nn.softmax(chosen, axis=-1)
    return jnp.sum(jnp.where(pick, share[:, :, None], 0.0), axis=1)


def mixer_half(
    mixer_input_channels,
    output_gate_logits,
    head_group_input_map,
    head_group_output_map,
    input_channel_taps,
    input_map_taps,
    output_map_taps,
    step_logits,
    head_log_rate,
    extra_log_decay,
    head_direct_scale,
    gated_norm_scale,
):
    length, width = mixer_input_channels.shape
    heads_dev = head_direct_scale.shape[0]
    head_dim = width // heads_dev
    group = lax.axis_index("tp") * heads_dev // (HEADS // GROUPS)
    first_col = group * STATE
    b_rows = lax.dynamic_slice_in_dim(head_group_input_map, first_col, STATE, 1)
    c_rows = lax.dynamic_slice_in_dim(head_group_output_map, first_col, STATE, 1)
    b_taps = lax.dynamic_slice_in_dim(input_map_taps, first_col, STATE, 1)
    c_taps = lax.dynamic_slice_in_dim(output_map_taps, first_col, STATE, 1)
    joined = jnp.concatenate([mixer_input_channels, b_rows, c_rows], axis=1)
    taps = jnp.concatenate([input_channel_taps, b_taps, c_taps], axis=1)
    reach = taps.shape[0] - 1
    before = from_behind(joined[length - reach :], "ep", 1)
    conv = conv_with_rows(joined, before, taps)
    nblk = length // BLOCK
    xs_f = conv[:, :width].astype(jnp.float32)
    bs_f = conv[:, width : width + STATE].astype(jnp.float32).reshape(nblk, BLOCK, STATE)
    cs_f = conv[:, width + STATE :].astype(jnp.float32).reshape(nblk, BLOCK, STATE)
    head_step_length = jax.nn.softplus(step_logits)
    position_log_decay = extra_log_decay - head_step_length * jnp.exp(head_log_rate)[:, None]
    cum = jnp.cumsum(position_log_decay.reshape(heads_dev, nblk, BLOCK), axis=2)
    step_blocks = jnp.transpose(head_step_length.reshape(heads_dev, nblk, BLOCK), (1, 2, 0))
    x_dt = xs_f.reshape(nblk, BLOCK, heads_dev, head_dim) * step_blocks[..., None]
    lower = jnp.tril(jnp.ones((BLOCK, BLOCK), bool))
    diff = cum[:, :, :, None] - cum[:, :, None, :]
    weight = jnp.where(lower, jnp.exp(jnp.where(lower, diff, 0.0)), 0.0)
    scores = jnp.einsum("bln,bsn->bls", cs_f, bs_f, precision=exact_prec)
    inner = jnp.einsum("bls,hbls,bshp->blhp", scores, weight, x_dt, precision=exact_prec)
    tail = jnp.exp(cum[:, :, -1:] - cum)
    block_state = jnp.einsum("bsn,hbs,bshp->bhpn", bs_f, tail, x_dt, precision=exact_prec)
    block_log = cum[:, :, -1]
    run_log = jnp.cumsum(block_log, axis=1)
    total_log = run_log[:, -1]
    own_state = jnp.einsum(
        "hb,bhpn->hpn", jnp.exp(total_log[:, None] - run_log), block_state, precision=exact_prec
    )
    own_decay = jnp.exp(total_log)
    entering = carried_in(own_state, own_decay, "ep")
    start_log = run_log - block_log
    earlier = jnp.arange(nblk)[:, None] > jnp.arange(nblk)[None, :]
    gap = start_log[:, :, None] - run_log[:, None, :]
    link = jnp.where(earlier, jnp.exp(jnp.where(earlier, gap, 0.0)), 0.0)
    prev = jnp.einsum("hbc,chpn->bhpn", link, block_state, precision=exact_prec)
    prev = prev + jnp.transpose(jnp.exp(start_log))[:, :, None, None] * entering[None]
    carried = jnp.einsum("bln,bhpn->blhp", cs_f, prev, precision=exact_prec)
    carried = carried * jnp.transpose(jnp.exp(cum), (1, 2, 0))[..., None]
    ssm = (inner + carried).reshape(length, heads_dev, head_dim)
    gated = (
        ssm + head_direct_scale[None, :, None] * xs_f.reshape(length, heads_dev, head_dim)
    ) * jax.nn.silu(output_gate_logits.astype(jnp.float32)).reshape(length, heads_dev, head_dim)
    gated = gated * lax.rsqrt(jnp.mean(gated * gated, axis=-1, keepdims=True) + eps)
    mixed = (gated.reshape(length, width) * gated_norm_scale.astype(jnp.float32)).astype(
        jnp.bfloat16
    )
    return rows_by_owner(mixed)


def project(rows_from, out_weight):
    n_ep = lax.axis_size("ep")
    place = lax.axis_index("ep")
    parts = jnp.einsum("rk,ekn->ern", rows_from, out_weight, preferred_element_type=jnp.float32)
    parts = parts.astype(jnp.bfloat16)
    ordered = [
        lax.dynamic_index_in_dim(parts, lax.rem(place + n_ep - q, n_ep), 0, False)
        for q in range(n_ep)
    ]
    return jnp.concatenate(ordered, axis=1)


def tp_moves():
    n_tp = lax.axis_size("tp")
    moves = []
    for flip in range(CORES):
        for level in range(n_tp // CORES):
            target = [(s // CORES + level) * CORES % n_tp + (s % CORES + flip) % CORES for s in range(n_tp)]
            moves.append((level, flip, target))
    return moves


def rows_by_owner(mixed):
    n_tp = lax.axis_size("tp")
    share = mixed.shape[0] // n_tp
    me = lax.axis_index("tp")
    got = []
    for level, flip, target in tp_moves():
        to = (me // CORES + level) * CORES % n_tp + (me % CORES + flip) % CORES
        piece = lax.dynamic_slice_in_dim(mixed, to * share, share, 0)
        if level or flip:
            piece = lax.ppermute(piece, "tp", list(enumerate(target)))
        got.append(piece)
    return jnp.concatenate(got, axis=1)


def out_weight_parts(weight):
    n_ep = lax.axis_size("ep")
    part = weight.shape[1] // n_ep
    own = lax.dynamic_slice_in_dim(weight, lax.axis_index("ep") * part, part, 1)
    levels = [
        lax.ppermute(own, "tp", list(enumerate(target))) if level else own
        for level, flip, target in tp_moves()
        if not flip
    ]
    column = jnp.concatenate(levels, axis=0)
    here = jnp.stack([column] + [ring_shift(column, "ep", k) for k in range(1, n_ep)])
    there = lax.ppermute(here, "tp", list(enumerate(s ^ 1 for s in range(lax.axis_size("tp")))))
    return jnp.concatenate([here, there], axis=1)


def expert_half(
    second_batch_tokens,
    pre_expert_norm_scale,
    group_router_columns,
    expert_router_columns,
    routes,
    expert_gate_weight,
    expert_up_weight,
    expert_down_weight,
):
    n_ep, n_tp = lax.axis_size("ep"), lax.axis_size("tp")
    n_tok, width = second_batch_tokens.shape
    n_experts = expert_router_columns.shape[1]
    cores = CORES
    share = n_tok // cores
    core = lax.axis_index("tp") % cores
    first = core * share
    tokens_f = lax.dynamic_slice_in_dim(second_batch_tokens, first, share, 0).astype(jnp.float32)
    own_routes = lax.dynamic_slice_in_dim(routes, first, share, 0)
    normed = (
        tokens_f
        * lax.rsqrt(jnp.mean(tokens_f * tokens_f, axis=-1, keepdims=True) + eps)
        * pre_expert_norm_scale.astype(jnp.float32)
    ).astype(jnp.bfloat16)
    group_logits = jnp.dot(normed, group_router_columns, preferred_element_type=jnp.float32)
    expert_logits = jnp.dot(normed, expert_router_columns, preferred_element_type=jnp.float32)
    weights = route_weights(group_logits, expert_logits, own_routes)
    coarse = lax.reduce_precision(weights, 8, 7)
    extra = jnp.concatenate([coarse, weights - coarse], axis=1).astype(jnp.bfloat16)
    extra = jnp.pad(extra, ((0, 0), (0, -extra.shape[1] % 128)))
    own = jnp.concatenate([normed, extra], axis=1)
    here = jnp.concatenate([own] + [ring_shift(own, "ep", k) for k in range(1, n_ep)], axis=0)
    there = lax.ppermute(here, "tp", [(s, s ^ 1) for s in range(n_tp)])
    low = jnp.where(core == 0, here, there)
    high = jnp.where(core == 0, there, here)
    rows = jnp.concatenate([low, high], axis=0)
    expert = lax.axis_index("ep")
    pair = rows[:, width : width + 2 * n_experts].astype(jnp.float32)
    wanted = jnp.arange(2 * n_experts) % n_experts == expert
    weight = jnp.sum(jnp.where(wanted, pair, 0.0), axis=1, keepdims=True)
    rows = rows[:, :width]
    gate = jnp.dot(rows, expert_gate_weight[0], preferred_element_type=jnp.float32)
    upper = jnp.dot(rows, expert_up_weight[0], preferred_element_type=jnp.float32)
    hidden = (jax.nn.silu(gate) * upper).astype(jnp.bfloat16)
    down = expert_down_weight[0]
    partial_sums = lax.dot_general(
        down, hidden, (((0,), (1,)), ((), ())), preferred_element_type=jnp.float32
    )
    partial_sums = (partial_sums * weight[:, 0][None, :]).astype(jnp.bfloat16)
    summed = lax.psum_scatter(partial_sums, "tp", scatter_dimension=0, tiled=True)
    blocks = summed.reshape(summed.shape[0], cores, n_ep, share)
    total = blocks[:, :, 0].astype(jnp.float32)
    for k in range(1, n_ep):
        total = total + ring_shift(blocks[:, :, k], "ep", -k).astype(jnp.float32)
    combined = total.reshape(summed.shape[0], n_tok)
    return jnp.transpose(combined).astype(jnp.bfloat16)


def per_device(
    mixer_input_channels,
    output_gate_logits,
    head_group_input_map,
    head_group_output_map,
    input_channel_taps,
    input_map_taps,
    output_map_taps,
    step_logits,
    head_log_rate,
    extra_log_decay,
    head_direct_scale,
    gated_norm_scale,
    mixer_output_weight,
    second_batch_tokens,
    pre_expert_norm_scale,
    group_router_columns,
    expert_router_columns,
    routes,
    expert_gate_weight,
    expert_up_weight,
    expert_down_weight,
):
    out_weight = out_weight_parts(mixer_output_weight)
    rows_from = mixer_half(
        mixer_input_channels,
        output_gate_logits,
        head_group_input_map,
        head_group_output_map,
        input_channel_taps,
        input_map_taps,
        output_map_taps,
        step_logits,
        head_log_rate,
        extra_log_decay,
        head_direct_scale,
        gated_norm_scale,
    )
    experts_out = expert_half(
        second_batch_tokens,
        pre_expert_norm_scale,
        group_router_columns,
        expert_router_columns,
        routes,
        expert_gate_weight,
        expert_up_weight,
        expert_down_weight,
    )
    rows_from, experts_out = lax.optimization_barrier((rows_from, experts_out))
    return (project(rows_from, out_weight), experts_out)


def solution(mesh):
    in_specs = (
        P("ep", "tp"),
        P("ep", "tp"),
        P("ep", None),
        P("ep", None),
        P(None, "tp"),
        P(),
        P(),
        P("tp", "ep"),
        P("tp"),
        P("tp", "ep"),
        P("tp"),
        P("tp"),
        P("tp", None),
        P("ep", None),
        P(),
        P(),
        P(),
        P("ep", None),
        P("ep", None, "tp"),
        P("ep", None, "tp"),
        P("ep", "tp", None),
    )
    out_specs = (P(("ep", "tp"), None), P("ep", "tp"))
    return jax.shard_map(
        per_device, mesh=mesh, in_specs=in_specs, out_specs=out_specs, check_vma=False
    )
```

profile of v0, /device:TPU:0, one launch (start us, length us, event | category | flops | bytes accessed | tf_op | source)
XLA Modules:
  0.0 209.2 jit_solution(6471672990444439608)
XLA Ops:
  12.9 3.0 %collective-permute-start.18 = (bf16[128,2176]{1,0:T(8,128)(2,1)S(1)}, bf16[128,2176]{1,0:T(8,128)(2,1)S(1)}, u32[]{:S(2)}, u32[]{:S(2)}) collective-permute-start(bf16[128,2176]{1,0:T(8,128)(2,1)S(1)} %pad_maximum_fusion.4), channel_id=1, source_target_pairs={{0,8},{8,16},{16,24},{24,0},{1,9},{9,17},{17,25},{25,1},{2,10},{10... | collective-permute-start | bytes 1671176 | tf_op jit(solution)/shard_map/ppermute | solution.py:36
  18.9 11.5 %collective-permute-done.18 = bf16[128,2176]{1,0:T(8,128)(2,1)S(1)} collective-permute-done((bf16[128,2176]{1,0:T(8,128)(2,1)S(1)}, bf16[128,2176]{1,0:T(8,128)(2,1)S(1)}, u32[]{:S(2)}, u32[]{:S(2)}) %collective-permute-start.18) | collective-permute-done | bytes 557088 | tf_op jit(solution)/shard_map/ppermute | solution.py:36
  30.4 11.0 %collective-permute-done.19 = bf16[128,2176]{1,0:T(8,128)(2,1)S(1)} collective-permute-done((bf16[128,2176]{1,0:T(8,128)(2,1)S(1)}, bf16[128,2176]{1,0:T(8,128)(2,1)S(1)}, u32[]{:S(2)}, u32[]{:S(2)}) %collective-permute-start.19) | collective-permute-done | bytes 557088 | tf_op jit(solution)/shard_map/ppermute | solution.py:36
  41.7 4.3 %pad_maximum_fusion.1 = bf16[512,2176]{1,0:T(8,128)(2,1)} fusion(bf16[128,2176]{1,0:T(8,128)(2,1)S(1)} %collective-permute-done.20, bf16[128,2176]{1,0:T(8,128)(2,1)S(1)} %collective-permute-done.19, bf16[128,2176]{1,0:T(8,128)(2,1)S(1)} %collective-permute-done.18, bf16[128,128]{1,0:T(8,128)(2,1)S(1)} %pad.4.clone, bf16[128,2048]{1,0:T(8,128)(2,1)S(1)} %fusion.58), kind=kLoop, calls=%fused_computation.32 | loop fusion | flops 11141120 | bytes 4456448 | tf_op jit(solution)/shard_map/concatenate | solution.py:216
  49.5 2.6 %collective-permute-start.1 = (bf16[256,512]{0,1:T(8,128)(2,1)}, bf16[256,512]{0,1:T(8,128)(2,1)}, u32[]{:S(2)}, u32[]{:S(2)}) collective-permute-start(bf16[256,512]{0,1:T(8,128)(2,1)} %copy.156), channel_id=1, source_target_pairs={{0,4},{1,5},{2,6},{3,7},{4,0},{5,1},{6,2},{7,3},{8,12},{9,13},{10,... | collective-permute-start | bytes 786440 | tf_op jit(solution)/shard_map/ppermute | solution.py:175
  53.4 2.3 %constant_dynamic-slice_fusion.8 = (bf16[2048,64]{1,0:T(8,128)(2,1)}, bf16[2048,64]{1,0:T(8,128)(2,1)S(1)}) fusion(bf16[2048,256]{1,0:T(8,128)(2,1)} %param.24, s32[]{:T(128)S(6)} %select_n.186, bf16[2048,256]{1,0:T(8,128)(2,1)} %param.23), kind=kLoop, calls=%fused_computation.157 | loop fusion | bytes 1048580 | tf_op jit(solution)/shard_map/dynamic_slice | solution.py:83
  57.3 2.3 %copy.124 = bf16[2048,256]{0,1:T(8,128)(2,1)} copy(bf16[2048,256]{1,0:T(8,128)(2,1)} %param.21) | data formatting | bytes 2097152 | tf_op args[0]
  60.5 4.3 %collective-permute-start.7 = (bf16[3,384]{0,1:T(8,128)(2,1)S(1)}, bf16[3,384]{0,1:T(8,128)(2,1)}, u32[]{:S(2)}, u32[]{:S(2)}) collective-permute-start(bf16[3,384]{0,1:T(8,128)(2,1)S(1)} %pad_maximum_fusion.6), channel_id=1, source_target_pairs={{0,8},{8,16},{16,24},{1,9},{9,17},{17,25},{2,10},{10,18},{18,26},{... | collective-permute-start | bytes 6920 | tf_op jit(solution)/shard_map/ppermute | solution.py:20
  66.2 4.6 %broadcast_select_fusion.1 = (bf16[512,2176]{1,0:T(8,128)(2,1)S(1)}, bf16[512,2176]{1,0:T(8,128)(2,1)S(1)}) fusion(bf16[512,2176]{1,0:T(8,128)(2,1)} %collective-permute-done.21, pred[]{:T(512)S(6)} %eq.51, bf16[128,2176]{1,0:T(8,128)(2,1)} %copy-done.8, bf16[128,2176]{1,0:T(8,128)(2,1)} %copy-done.7, bf16[128,2176]{1,0:T(8,128)(2,1)} %copy-done.6, ...), kind=kLoop, calls=%fused_computation.34 | loop fusion | flops 13369344 | bytes 8912897 | tf_op jit(solution)/shard_map/jit(_where)/select_n | solution.py:218
  70.8 4.3 %fusion.32 = f32[1024,512]{1,0:T(8,128)} fusion(bf16[1,2048,512]{2,1,0:T(8,128)(2,1)S(1)} %copy-done.25, bf16[512,2176]{1,0:T(8,128)(2,1)S(1)} %get-tuple-element.22, bf16[512,2176]{1,0:T(8,128)(2,1)S(1)} %get-tuple-element.23), kind=kOutput, calls=%fused_computation.48 | convolution fusion | flops 2155872256 | bytes 8650752 | tf_op jit(solution)/shard_map/dot_general | solution.py:227
  75.3 8.9 %fusion.17 = bf16[2048,1024]{0,1:T(8,128)(2,1)} fusion(f32[1024]{0:T(1024)S(1)} %select_reduce_fusion, bf16[1,512,2048]{2,1,0:T(8,128)(2,1)S(1)} %copy-done, f32[1024,512]{1,0:T(8,128)} %fusion.32, bf16[1,2048,512]{2,1,0:T(8,128)(2,1)} %param.39, bf16[512,2176]{1,0:T(8,128)(2,1)} %copy-done.3, bf16[512,2176]{1,0:T(8,128)(2,1)} %copy-done.4), kind=kOutput, calls=%fused_computation.21 | convolution fusion | flops 4310695936 | bytes 14946304 | tf_op jit(solution)/shard_map/dot_general | solution.py:230
  93.2 3.0 %multiply_convert_fusion.1 = bf16[2048,384]{0,1:T(8,128)(2,1)S(1)} fusion(f32[2051,384]{0,1:T(8,128)S(1)} %maximum_convert_fusion, f32[384]{0:T(512)S(1)} %get-tuple-element.17, f32[384]{0:T(512)S(1)} %get-tuple-element.18, f32[384]{0:T(512)S(1)} %get-tuple-element.19, f32[384]{0:T(512)S(1)} %get-tuple-element.16), kind=kLoop, calls=%fused_computation.29 | loop fusion | flops 9437184 | bytes 14161920 | tf_op jit(solution)/shard_map/convert_element_type | solution.py:45
  96.4 2.8 %fusion.108 = (bf16[1,1024,512]{1,2,0:T(8,128)(2,1)}, bf16[1024,512]{0,1:T(8,128)(2,1)}) fusion(bf16[256,512]{0,1:T(8,128)(2,1)} %collective-permute-done.2, bf16[256,512]{0,1:T(8,128)(2,1)} %collective-permute-done.1, bf16[256,512]{0,1:T(8,128)(2,1)} %collective-permute-done, bf16[256,512]{0,1:T(8,128)(2,1)} %copy.156), kind=kLoop, calls=%fused_computation.200 | loop fusion | flops 4194304 | bytes 3145728 | tf_op jit(solution)/shard_map/stack | solution.py:180
  110.1 3.1 %collective-permute-start.8 = (bf16[4,72,64]{1,2,0:T(8,128)(2,1)S(1)}, bf16[4,72,64]{1,2,0:T(8,128)(2,1)S(1)}, u32[]{:S(2)}, u32[]{:S(2)}) collective-permute-start(bf16[4,72,64]{1,2,0:T(8,128)(2,1)S(1)} %pad_maximum_fusion.8), channel_id=1, source_target_pairs={{0,24},{1,25},{2,26},{3,27},{4,28},{5,29},{6,30},{7,31}} | collective-permute-start | bytes 110600 | tf_op jit(solution)/shard_map/ppermute | solution.py:20
  114.5 12.0 %collective-permute-done.3 = bf16[1024,512]{0,1:T(8,128)(2,1)} collective-permute-done((bf16[1024,512]{0,1:T(8,128)(2,1)}, bf16[1024,512]{0,1:T(8,128)(2,1)}, u32[]{:S(2)}, u32[]{:S(2)}) %collective-permute-start.3) | collective-permute-done | bytes 1048608 | tf_op jit(solution)/shard_map/ppermute | solution.py:36
  128.7 18.3 %collective-permute-done.4 = bf16[1024,512]{0,1:T(8,128)(2,1)} collective-permute-done((bf16[1024,512]{0,1:T(8,128)(2,1)}, bf16[1024,512]{0,1:T(8,128)(2,1)}, u32[]{:S(2)}, u32[]{:S(2)}) %collective-permute-start.4) | collective-permute-done | bytes 1048608 | tf_op jit(solution)/shard_map/ppermute | solution.py:36
  147.0 3.8 %pad_maximum_fusion = bf16[4,1024,512]{1,2,0:T(8,128)(2,1)} fusion(bf16[1,1024,512]{1,2,0:T(8,128)(2,1)} %bitcast.3, bf16[1,1024,512]{1,2,0:T(8,128)(2,1)} %bitcast.2, bf16[1,1024,512]{1,2,0:T(8,128)(2,1)} %bitcast.1, bf16[1,1024,512]{1,2,0:T(8,128)(2,1)} %get-tuple-element.40), kind=kLoop, calls=%fused_computation.14 | loop fusion | flops 6291456 | bytes 8388608 | tf_op jit(solution)/shard_map/stack | solution.py:180
  151.2 3.3 %fusion.11 = f32[16,4,128,64]{2,3,1,0:T(8,128)} fusion(bf16[16,128,4,64]{1,0,3,2:T(8,128)(2,1)S(1)} %copy-done.10, f32[16,128,128]{2,1,0:T(8,128)S(1)} %fusion.66, f32[4,16,128]{2,0,1:T(4,128)S(1)} %copy-done.12, pred[128,128]{1,0:T(8,128)(4,1)S(1)} %copy-done.15), kind=kOutput, calls=%fused_computation.15 | convolution fusion | flops 138412032 | bytes 4243456 | tf_op jit(solution)/shard_map/bls,hbls,bshp->blhp/dot_general | solution.py:104
  163.3 2.8 %collective-permute-start.13 = (bf16[256,256]{0,1:T(8,128)(2,1)S(1)}, bf16[256,256]{0,1:T(8,128)(2,1)S(1)}, u32[]{:S(2)}, u32[]{:S(2)}) collective-permute-start(bf16[256,256]{0,1:T(8,128)(2,1)S(1)} %get-tuple-element.36), channel_id=1, source_target_pairs={{0,6},{1,7},{2,0},{3,1},{4,2},{5,3},{6,4},{7,5},{8,14},{9,15},{10,... | collective-permute-start | bytes 393224 | tf_op jit(solution)/shard_map/ppermute | solution.py:165
  166.2 4.5 %collective-permute-done.11 = bf16[256,256]{0,1:T(8,128)(2,1)S(1)} collective-permute-done((bf16[256,256]{0,1:T(8,128)(2,1)S(1)}, bf16[256,256]{0,1:T(8,128)(2,1)S(1)}, u32[]{:S(2)}, u32[]{:S(2)}) %collective-permute-start.11) | collective-permute-done | bytes 131104 | tf_op jit(solution)/shard_map/ppermute | solution.py:165
  170.7 5.5 %collective-permute-done.12 = bf16[256,256]{0,1:T(8,128)(2,1)S(1)} collective-permute-done((bf16[256,256]{0,1:T(8,128)(2,1)S(1)}, bf16[256,256]{0,1:T(8,128)(2,1)S(1)}, u32[]{:S(2)}, u32[]{:S(2)}) %collective-permute-start.12) | collective-permute-done | bytes 131104 | tf_op jit(solution)/shard_map/ppermute | solution.py:165
  179.5 4.3 %collective-permute-start.22 = (bf16[256,2,128]{0,2,1:T(8,128)(2,1)S(1)}, bf16[256,2,128]{0,2,1:T(8,128)(2,1)S(1)}, u32[]{:S(2)}, u32[]{:S(2)}) collective-permute-start(bf16[256,2,128]{0,2,1:T(8,128)(2,1)S(1)} %get-tuple-element.42), channel_id=1, source_target_pairs={{0,24},{8,0},{16,8},{24,16},{1,25},{9,1},{17,9},{25,17},{2,26},{10... | collective-permute-start | bytes 393224 | tf_op jit(solution)/shard_map/ppermute | solution.py:36
  189.7 4.8 %collective-permute-done.24 = bf16[256,2,128]{0,2,1:T(8,128)(2,1)S(1)} collective-permute-done((bf16[256,2,128]{0,2,1:T(8,128)(2,1)S(1)}, bf16[256,2,128]{0,2,1:T(8,128)(2,1)S(1)}, u32[]{:S(2)}, u32[]{:S(2)}) %collective-permute-start.24) | collective-permute-done | bytes 131104 | tf_op jit(solution)/shard_map/ppermute | solution.py:36
  196.2 4.5 %fusion.52 = bf16[4,512,256]{2,1,0:T(8,128)(2,1)S(1)} fusion(bf16[4,1024,512]{1,2,0:T(8,128)(2,1)} %collective-permute-done.6, bf16[1,1024,512]{1,2,0:T(8,128)(2,1)} %bitcast.3, bf16[1,1024,512]{1,2,0:T(8,128)(2,1)} %bitcast.2, bf16[1,1024,512]{1,2,0:T(8,128)(2,1)} %bitcast.1, bf16[1,1024,512]{1,2,0:T(8,128)(2,1)S(1)} %copy-done.5, ...), kind=kOutput, calls=%fused_computation.70 | convolution fusion | flops 2189950976 | bytes 10485760 | tf_op jit(solution)/shard_map/rk,ekn->ern/dot_general | solution.py:137
  (186 shorter events, 62.5 us)
Async XLA Ops:
  7.2 171.2 %reduce-scatter.2.cloned.1.call-start = ((), (), s32[]{:S(2)}) async-start(), calls=%async_computation.1 | async-start | bytes 4718592 | tf_op jit(solution)/shard_map/reduce_scatter | solution.py:234
  12.9 17.5 %collective-permute-start.18 = (bf16[128,2176]{1,0:T(8,128)(2,1)S(1)}, bf16[128,2176]{1,0:T(8,128)(2,1)S(1)}, u32[]{:S(2)}, u32[]{:S(2)}) collective-permute-start(bf16[128,2176]{1,0:T(8,128)(2,1)S(1)} %pad_maximum_fusion.4), channel_id=1, source_target_pairs={{0,8},{8,16},{16,24},{24,0},{1,9},{9,17},{17,25},{25,1},{2,10},{10... | collective-permute-start | bytes 1671176 | tf_op jit(solution)/shard_map/ppermute | solution.py:36
  15.9 25.5 %collective-permute-start.19 = (bf16[128,2176]{1,0:T(8,128)(2,1)S(1)}, bf16[128,2176]{1,0:T(8,128)(2,1)S(1)}, u32[]{:S(2)}, u32[]{:S(2)}) collective-permute-start(bf16[128,2176]{1,0:T(8,128)(2,1)S(1)} %pad_maximum_fusion.4), channel_id=1, source_target_pairs={{0,16},{8,24},{16,0},{24,8},{1,17},{9,25},{17,1},{25,9},{2,18},{10... | collective-permute-start | bytes 1671176 | tf_op jit(solution)/shard_map/ppermute | solution.py:36
  17.4 24.3 %collective-permute-start.20 = (bf16[128,2176]{1,0:T(8,128)(2,1)S(1)}, bf16[128,2176]{1,0:T(8,128)(2,1)S(1)}, u32[]{:S(2)}, u32[]{:S(2)}) collective-permute-start(bf16[128,2176]{1,0:T(8,128)(2,1)S(1)} %pad_maximum_fusion.4), channel_id=1, source_target_pairs={{0,24},{8,0},{16,8},{24,16},{1,25},{9,1},{17,9},{25,17},{2,26},{10... | collective-permute-start | bytes 1671176 | tf_op jit(solution)/shard_map/ppermute | solution.py:36
  46.0 20.2 %collective-permute-start.21 = (bf16[512,2176]{1,0:T(8,128)(2,1)}, bf16[512,2176]{1,0:T(8,128)(2,1)}, u32[]{:S(2)}, u32[]{:S(2)}) collective-permute-start(bf16[512,2176]{1,0:T(8,128)(2,1)} %pad_maximum_fusion.1), channel_id=1, source_target_pairs={{0,1},{1,0},{2,3},{3,2},{4,5},{5,4},{6,7},{7,6},{8,9},{9,8},{10,11... | collective-permute-start | bytes 6684680 | tf_op jit(solution)/shard_map/ppermute | solution.py:217
  47.9 48.5 %collective-permute-start = (bf16[256,512]{0,1:T(8,128)(2,1)}, bf16[256,512]{0,1:T(8,128)(2,1)}, u32[]{:S(2)}, u32[]{:S(2)}) collective-permute-start(bf16[256,512]{0,1:T(8,128)(2,1)} %copy.156), channel_id=1, source_target_pairs={{0,2},{1,3},{2,4},{3,5},{4,6},{5,7},{6,0},{7,1},{8,10},{9,11},{10,... | collective-permute-start | bytes 786440 | tf_op jit(solution)/shard_map/ppermute | solution.py:175
  49.5 46.9 %collective-permute-start.1 = (bf16[256,512]{0,1:T(8,128)(2,1)}, bf16[256,512]{0,1:T(8,128)(2,1)}, u32[]{:S(2)}, u32[]{:S(2)}) collective-permute-start(bf16[256,512]{0,1:T(8,128)(2,1)} %copy.156), channel_id=1, source_target_pairs={{0,4},{1,5},{2,6},{3,7},{4,0},{5,1},{6,2},{7,3},{8,12},{9,13},{10,... | collective-permute-start | bytes 786440 | tf_op jit(solution)/shard_map/ppermute | solution.py:175
  52.1 44.4 %collective-permute-start.2 = (bf16[256,512]{0,1:T(8,128)(2,1)}, bf16[256,512]{0,1:T(8,128)(2,1)}, u32[]{:S(2)}, u32[]{:S(2)}) collective-permute-start(bf16[256,512]{0,1:T(8,128)(2,1)} %copy.156), channel_id=1, source_target_pairs={{0,6},{1,7},{2,0},{3,1},{4,2},{5,3},{6,4},{7,5},{8,14},{9,15},{10,... | collective-permute-start | bytes 786440 | tf_op jit(solution)/shard_map/ppermute | solution.py:175
  60.5 31.2 %collective-permute-start.7 = (bf16[3,384]{0,1:T(8,128)(2,1)S(1)}, bf16[3,384]{0,1:T(8,128)(2,1)}, u32[]{:S(2)}, u32[]{:S(2)}) collective-permute-start(bf16[3,384]{0,1:T(8,128)(2,1)S(1)} %pad_maximum_fusion.6), channel_id=1, source_target_pairs={{0,8},{8,16},{16,24},{1,9},{9,17},{17,25},{2,10},{10,18},{18,26},{... | collective-permute-start | bytes 6920 | tf_op jit(solution)/shard_map/ppermute | solution.py:20
  99.2 27.2 %collective-permute-start.3 = (bf16[1024,512]{0,1:T(8,128)(2,1)}, bf16[1024,512]{0,1:T(8,128)(2,1)}, u32[]{:S(2)}, u32[]{:S(2)}) collective-permute-start(bf16[1024,512]{0,1:T(8,128)(2,1)} %get-tuple-element.41), channel_id=1, source_target_pairs={{0,8},{8,16},{16,24},{24,0},{1,9},{9,17},{17,25},{25,1},{2,10},{10... | collective-permute-start | bytes 3145736 | tf_op jit(solution)/shard_map/ppermute | solution.py:36
  100.0 46.9 %collective-permute-start.4 = (bf16[1024,512]{0,1:T(8,128)(2,1)}, bf16[1024,512]{0,1:T(8,128)(2,1)}, u32[]{:S(2)}, u32[]{:S(2)}) collective-permute-start(bf16[1024,512]{0,1:T(8,128)(2,1)} %get-tuple-element.41), channel_id=1, source_target_pairs={{0,16},{8,24},{16,0},{24,8},{1,17},{9,25},{17,1},{25,9},{2,18},{10... | collective-permute-start | bytes 3145736 | tf_op jit(solution)/shard_map/ppermute | solution.py:36
  100.0 46.9 %collective-permute-start.5 = (bf16[1024,512]{0,1:T(8,128)(2,1)}, bf16[1024,512]{0,1:T(8,128)(2,1)}, u32[]{:S(2)}, u32[]{:S(2)}) collective-permute-start(bf16[1024,512]{0,1:T(8,128)(2,1)} %get-tuple-element.41), channel_id=1, source_target_pairs={{0,24},{8,0},{16,8},{24,16},{1,25},{9,1},{17,9},{25,17},{2,26},{10... | collective-permute-start | bytes 3145736 | tf_op jit(solution)/shard_map/ppermute | solution.py:36
  110.1 44.5 %collective-permute-start.8 = (bf16[4,72,64]{1,2,0:T(8,128)(2,1)S(1)}, bf16[4,72,64]{1,2,0:T(8,128)(2,1)S(1)}, u32[]{:S(2)}, u32[]{:S(2)}) collective-permute-start(bf16[4,72,64]{1,2,0:T(8,128)(2,1)S(1)} %pad_maximum_fusion.8), channel_id=1, source_target_pairs={{0,24},{1,25},{2,26},{3,27},{4,28},{5,29},{6,30},{7,31}} | collective-permute-start | bytes 110600 | tf_op jit(solution)/shard_map/ppermute | solution.py:20
  113.2 41.3 %collective-permute-start.10 = (bf16[4,72,64]{1,2,0:T(8,128)(2,1)S(1)}, bf16[4,72,64]{1,2,0:T(8,128)(2,1)S(1)}, u32[]{:S(2)}, u32[]{:S(2)}) collective-permute-start(bf16[4,72,64]{1,2,0:T(8,128)(2,1)S(1)} %pad_maximum_fusion.8), channel_id=1, source_target_pairs={{0,8},{8,16},{16,24},{1,9},{9,17},{17,25},{2,10},{10,18},{18,26},{... | collective-permute-start | bytes 110600 | tf_op jit(solution)/shard_map/ppermute | solution.py:20
  126.5 28.1 %collective-permute-start.9 = (bf16[4,72,64]{1,2,0:T(8,128)(2,1)S(1)}, bf16[4,72,64]{1,2,0:T(8,128)(2,1)S(1)}, u32[]{:S(2)}, u32[]{:S(2)}) collective-permute-start(bf16[4,72,64]{1,2,0:T(8,128)(2,1)S(1)} %pad_maximum_fusion.8), channel_id=1, source_target_pairs={{0,16},{8,24},{1,17},{9,25},{2,18},{10,26},{3,19},{11,27},{4,20},{... | collective-permute-start | bytes 110600 | tf_op jit(solution)/shard_map/ppermute | solution.py:20
  150.8 45.4 %collective-permute-start.6 = (bf16[4,1024,512]{1,2,0:T(8,128)(2,1)}, bf16[4,1024,512]{1,2,0:T(8,128)(2,1)}, u32[]{:S(2)}, u32[]{:S(2)}) collective-permute-start(bf16[4,1024,512]{1,2,0:T(8,128)(2,1)} %pad_maximum_fusion), channel_id=1, source_target_pairs={{0,1},{1,0},{2,3},{3,2},{4,5},{5,4},{6,7},{7,6},{8,9},{9,8},{10,11... | collective-permute-start | bytes 12582920 | tf_op jit(solution)/shard_map/ppermute | solution.py:181
  162.3 8.4 %collective-permute-start.11 = (bf16[256,256]{0,1:T(8,128)(2,1)S(1)}, bf16[256,256]{0,1:T(8,128)(2,1)S(1)}, u32[]{:S(2)}, u32[]{:S(2)}) collective-permute-start(bf16[256,256]{0,1:T(8,128)(2,1)S(1)} %get-tuple-element.38), channel_id=1, source_target_pairs={{0,2},{1,3},{2,4},{3,5},{4,6},{5,7},{6,0},{7,1},{8,10},{9,11},{10,... | collective-permute-start | bytes 393224 | tf_op jit(solution)/shard_map/ppermute | solution.py:165
  163.1 13.1 %collective-permute-start.12 = (bf16[256,256]{0,1:T(8,128)(2,1)S(1)}, bf16[256,256]{0,1:T(8,128)(2,1)S(1)}, u32[]{:S(2)}, u32[]{:S(2)}) collective-permute-start(bf16[256,256]{0,1:T(8,128)(2,1)S(1)} %get-tuple-element.37), channel_id=1, source_target_pairs={{0,4},{1,5},{2,6},{3,7},{4,0},{5,1},{6,2},{7,3},{8,12},{9,13},{10,... | collective-permute-start | bytes 393224 | tf_op jit(solution)/shard_map/ppermute | solution.py:165
  163.3 12.8 %collective-permute-start.13 = (bf16[256,256]{0,1:T(8,128)(2,1)S(1)}, bf16[256,256]{0,1:T(8,128)(2,1)S(1)}, u32[]{:S(2)}, u32[]{:S(2)}) collective-permute-start(bf16[256,256]{0,1:T(8,128)(2,1)S(1)} %get-tuple-element.36), channel_id=1, source_target_pairs={{0,6},{1,7},{2,0},{3,1},{4,2},{5,3},{6,4},{7,5},{8,14},{9,15},{10,... | collective-permute-start | bytes 393224 | tf_op jit(solution)/shard_map/ppermute | solution.py:165
  166.2 12.1 %collective-permute-start.14 = (bf16[256,256]{0,1:T(8,128)(2,1)S(1)}, bf16[256,256]{0,1:T(8,128)(2,1)S(1)}, u32[]{:S(2)}, u32[]{:S(2)}) collective-permute-start(bf16[256,256]{0,1:T(8,128)(2,1)S(1)} %get-tuple-element.35), channel_id=1, source_target_pairs={{0,1},{1,0},{2,3},{3,2},{4,5},{5,4},{6,7},{7,6},{8,9},{9,8},{10,11... | collective-permute-start | bytes 393224 | tf_op jit(solution)/shard_map/ppermute | solution.py:165
  176.1 9.9 %collective-permute-start.16 = (bf16[256,256]{0,1:T(8,128)(2,1)S(1)}, bf16[256,256]{0,1:T(8,128)(2,1)S(1)}, u32[]{:S(2)}, u32[]{:S(2)}) collective-permute-start(bf16[256,256]{0,1:T(8,128)(2,1)S(1)} %get-tuple-element.33), channel_id=1, source_target_pairs={{0,5},{1,4},{2,7},{3,6},{4,1},{5,0},{6,3},{7,2},{8,13},{9,12},{10,... | collective-permute-start | bytes 393224 | tf_op jit(solution)/shard_map/ppermute | solution.py:165
  176.2 13.0 %collective-permute-start.17 = (bf16[256,256]{0,1:T(8,128)(2,1)S(1)}, bf16[256,256]{0,1:T(8,128)(2,1)S(1)}, u32[]{:S(2)}, u32[]{:S(2)}) collective-permute-start(bf16[256,256]{0,1:T(8,128)(2,1)S(1)} %get-tuple-element.32), channel_id=1, source_target_pairs={{0,7},{1,6},{2,1},{3,0},{4,3},{5,2},{6,5},{7,4},{8,15},{9,14},{10,... | collective-permute-start | bytes 393224 | tf_op jit(solution)/shard_map/ppermute | solution.py:165
  179.5 9.8 %collective-permute-start.22 = (bf16[256,2,128]{0,2,1:T(8,128)(2,1)S(1)}, bf16[256,2,128]{0,2,1:T(8,128)(2,1)S(1)}, u32[]{:S(2)}, u32[]{:S(2)}) collective-permute-start(bf16[256,2,128]{0,2,1:T(8,128)(2,1)S(1)} %get-tuple-element.42), channel_id=1, source_target_pairs={{0,24},{8,0},{16,8},{24,16},{1,25},{9,1},{17,9},{25,17},{2,26},{10... | collective-permute-start | bytes 393224 | tf_op jit(solution)/shard_map/ppermute | solution.py:36
  186.0 8.5 %collective-permute-start.24 = (bf16[256,2,128]{0,2,1:T(8,128)(2,1)S(1)}, bf16[256,2,128]{0,2,1:T(8,128)(2,1)S(1)}, u32[]{:S(2)}, u32[]{:S(2)}) collective-permute-start(bf16[256,2,128]{0,2,1:T(8,128)(2,1)S(1)} %get-tuple-element.43), channel_id=1, source_target_pairs={{0,8},{8,16},{16,24},{24,0},{1,9},{9,17},{17,25},{25,1},{2,10},{10... | collective-permute-start | bytes 393224 | tf_op jit(solution)/shard_map/ppermute | solution.py:36
  (30 other events, 244.2 us)
Sparse Core Ops, SparseCore 0:
  84.4 46.6 reduce-scatter.1
where the time goes:
time: 211 us; the launch traced here: 209 us
  waiting for transfers between devices  71.6 us (34%)
  starting transfers between devices  38.1 us (18%)
  other arithmetic  37.1 us (18%)
  matrix products  29.3 us (14%)
  local copies, waits for them, and re-layouts  18.2 us (9%)
  between operations  14.8 us (7%)
    ppermute x9, waiting for transfers between devices, ring_shift(): lax.ppermute(value, axis, [(s, (s + steps) % count) for s in range(count)])  58.4 us
    ppermute x9, starting transfers between devices, ring_shift(): lax.ppermute(value, axis, [(s, (s + steps) % count) for s in range(count)])  15.5 us
    ppermute x7, waiting for transfers between devices, rows_by_owner(): piece = lax.ppermute(piece, 'tp', list(enumerate(target)))  13.1 us
    ppermute x4, starting transfers between devices, from_behind(): lax.ppermute(value, axis, [(source, source + steps) for source in range(f...  10.9 us
    dot_general x1, matrix products, expert_half(): lax.dot_general(down, hidden, (((0,), (1,)), ((), ())), preferred_element...  8.94 us
    unnamed x73, local copies, waits for them, and re-layouts  8.53 us
    another operation x2, other arithmetic, out_weight_parts(): jnp.stack([column] + [ring_shift(column, 'ep', k) for k in range(1, n_ep)])  6.59 us
    ppermute x7, starting transfers between devices, rows_by_owner(): piece = lax.ppermute(piece, 'tp', list(enumerate(target)))  6 us
  transfers between devices with their start and end apart: 26, of which 11 were waited for; matrix products, arithmetic and copies ran while one was open for 33% of the time, Pallas kernels for 0%

commit v1 on v0

v1 whole, which is shorter than its diff:
```python
import functools
import math

import jax
import jax.numpy as jnp
from jax import lax
from jax.experimental import pallas as pl
from jax.experimental.pallas import tpu as pltpu
from jax.sharding import PartitionSpec as P

STATE = 64
GROUPS = 4
HEADS = 32
BLOCK = 128
CORES = 2
LANES = 128
HALO = 16
EPS = 1e-6
MESH = pl.DeviceIdType.MESH
F32 = jnp.float32
BF16 = jnp.bfloat16


def snake(i, n):
    w = math.isqrt(n)
    y, x = i // w, i % w
    odd = y % 2
    return y * w + x * (1 - 2 * odd) + odd * (w - 1)


def silu(v):
    return v / (1.0 + jnp.exp(-v))


def dot(a, b, dims=(((1,), (0,)), ((), ()))):
    return lax.dot_general(a, b, dims, preferred_element_type=F32)


def kernel(
    n_ep,
    n_tp,
    x_hbm,
    gate_hbm,
    b_hbm,
    c_hbm,
    wout_hbm,
    tok_hbm,
    eg_hbm,
    eu_hbm,
    ed_hbm,
    xtaps,
    btaps,
    ctaps,
    step,
    extra,
    lograte,
    dscale,
    gnorm,
    pnorm,
    router,
    routes,
    out,
    eout,
    xpad,
    bcpad,
    gate,
    eg,
    eu,
    ed,
    wk,
    rows_tok,
    wts,
    hid,
    psend,
    pmine,
    precv,
    rsrecv,
    zsend,
    zrecv,
    xs_s,
    bc_s,
    rows_s,
    prev_s,
    dpre_s,
    st_s,
    dec_s,
    smsg,
    srecv,
    ent,
    mixed,
    mrecv,
    pjsend,
    pjown,
    pjrecv,
    ld,
    halo_s,
    halo_r,
    tok_s,
    tok_r,
    tokp_s,
    tokp_r,
    wts_s,
    wts_r,
    wz_s,
    wz_r,
    wr_s,
    wr_r,
    state_s,
    state_r,
    pd_s,
    pd_r,
    rs_s,
    rs_r,
    zs_s,
    zs_r,
    a2a_s,
    a2a_r,
    pj_s,
    pj_r,
):
    n_z = n_tp // CORES
    half_ring = n_ep // 2
    e = lax.axis_index("ep")
    t = lax.axis_index("tp")
    c = t % CORES
    z = t // CORES
    ring = snake(e, n_ep)
    partner = (e, t + 1 - 2 * c)

    def at_ring(offset):
        return snake((ring + offset + n_ep) % n_ep, n_ep)

    next_ep, prev_ep = at_ring(1), at_ring(-1)
    toward = ((next_ep, t), (prev_ep, t))
    length, width = x_hbm.shape
    heads = width // STATE
    nblk = length // BLOCK
    group = t * heads // (HEADS // GROUPS)
    pair = group * STATE // LANES
    within = group * STATE % LANES
    n_tok, depth = tok_hbm.shape
    half = n_tok // CORES
    quarter = half // 2
    feats = depth // n_tp
    ff = eg_hbm.shape[1]
    rows_w = wout_hbm.shape[0]
    part = wout_hbm.shape[1] // n_ep
    rows_dev = out.shape[0]
    n_experts = n_ep
    pending = []

    def remote(src, dst, send, recv, device):
        return pltpu.make_async_remote_copy(
            src_ref=src, dst_ref=dst, send_sem=send, recv_sem=recv, device_id=device, device_id_type=MESH
        )

    def send(src, dst, send_sem, recv_sem, device):
        copy = remote(src, dst, send_sem, recv_sem, device)
        copy.start()
        pending.append(copy)
        return copy

    def arrived(view, sem):
        remote(view, view, sem, sem, partner).wait_recv()

    def local(src, dst, index):
        copy = pltpu.make_async_copy(src, dst, ld.at[index])
        copy.start()
        return copy

    get_tok = local(tok_hbm, rows_tok.at[e], 0)
    get_eg = local(eg_hbm, eg, 1)
    get_eu = local(eu_hbm, eu, 2)
    get_ed = local(ed_hbm, ed, 3)
    lane_b = pl.ds(pl.multiple_of(pair * LANES, LANES), LANES)
    get_x = local(x_hbm, xpad.at[pl.ds(HALO, length)], 4)
    get_b = local(b_hbm.at[:, lane_b], bcpad.at[pl.ds(HALO, length), pl.ds(0, LANES)], 5)
    get_c = local(c_hbm.at[:, lane_b], bcpad.at[pl.ds(HALO, length), pl.ds(LANES, LANES)], 6)
    get_gate = local(gate_hbm, gate, 7)
    get_w = [
        local(wout_hbm.at[:, pl.ds(q * part, part)], wk.at[q, z], 8 + q) for q in range(n_ep)
    ]

    barrier = pltpu.get_barrier_semaphore()
    peers = 0
    for k in range(1, n_ep):
        pl.semaphore_signal(barrier, inc=1, device_id=((e + k) % n_ep, t), device_id_type=MESH)
        peers += 1
    for k in range(1, n_z):
        pl.semaphore_signal(
            barrier, inc=1, device_id=(e, (t + CORES * k) % n_tp), device_id_type=MESH
        )
        peers += 1
    pl.semaphore_signal(barrier, inc=1, device_id=partner, device_id_type=MESH)
    peers += 1

    get_tok.wait()
    scale = pnorm[...].astype(F32)

    def norm_rows(i, carry):
        rows = pl.ds(pl.multiple_of(i * 32, 32), 32)
        v = rows_tok[e, rows, :].astype(F32)
        v = v * lax.rsqrt(jnp.mean(v * v, axis=-1, keepdims=True) + EPS) * scale
        rows_tok[e, rows, :] = v.astype(BF16)
        return carry

    lax.fori_loop(0, n_tok // 32, norm_rows, 0)

    pl.semaphore_wait(barrier, peers)

    def tok_rows(core, way, last):
        if last:
            return pl.ds(pl.multiple_of(core * half + way * quarter, quarter), quarter)
        return pl.ds(pl.multiple_of(core * half, half), half)

    def send_tokens(way, d):
        block = at_ring(-(d - 1) if way == 0 else d - 1)
        view = rows_tok.at[block, tok_rows(c, way, d == half_ring), :]
        send(view, view, tok_s.at[way, d - 1], tok_r.at[way, d - 1], toward[way])

    def share_tokens(way, d):
        block = at_ring(-d if way == 0 else d)
        view = rows_tok.at[block, tok_rows(c, way, d == half_ring), :]
        arrived(view, tok_r.at[way, d - 1])
        if d < half_ring:
            send_tokens(way, d + 1)
        send(view, view, tokp_s.at[way, d - 1], tokp_r.at[way, d - 1], partner)

    def shared_tokens(way, d):
        block = at_ring(-d if way == 0 else d)
        view = rows_tok.at[block, tok_rows(1 - c, way, d == half_ring), :]
        arrived(view, tokp_r.at[way, d - 1])

    for way in range(2):
        send_tokens(way, 1)

    tail_rows = pl.ds(length - HALO, HALO)
    head_rows = pl.ds(0, HALO)
    halo = [
        remote(src, dst, halo_s.at[i], halo_r.at[i], ((e + 1) % n_ep, t))
        for i, (src, dst) in enumerate(
            (
                (x_hbm.at[tail_rows], xpad.at[head_rows]),
                (b_hbm.at[tail_rows, lane_b], bcpad.at[head_rows, pl.ds(0, LANES)]),
                (c_hbm.at[tail_rows, lane_b], bcpad.at[head_rows, pl.ds(LANES, LANES)]),
            )
        )
    ]

    @pl.when(e < n_ep - 1)
    def _():
        for copy in halo:
            copy.start()

    @pl.when(e == 0)
    def _():
        xpad[head_rows, :] = jnp.zeros((HALO, width), BF16)
        bcpad[head_rows, :] = jnp.zeros((HALO, 2 * LANES), BF16)

    mine = pl.ds(pl.multiple_of(e * part, part), part)
    for k in range(1, n_z):
        send(
            wout_hbm.at[:, mine],
            wk.at[e, z],
            wz_s.at[k - 1],
            wz_r.at[k - 1],
            (e, (t + CORES * k) % n_tp),
        )

    logits = dot(router[...], rows_tok[e], (((1,), (1,)), ((), ())))
    expert_logit = [logits[i : i + 1, :] for i in range(n_experts)]
    n_grp = max(1, n_experts // 4)
    per_group = n_experts // n_grp
    group_logit = [logits[n_experts + i : n_experts + i + 1, :] for i in range(n_grp)]

    def log_softmax(rows):
        top = functools.reduce(jnp.maximum, rows)
        norm = jnp.log(functools.reduce(jnp.add, [jnp.exp(v - top) for v in rows]))
        return [v - top - norm for v in rows]

    group_lp = log_softmax(group_logit)
    total_lp = []
    for i in range(n_grp):
        inner = log_softmax(expert_logit[i * per_group : (i + 1) * per_group])
        total_lp += [group_lp[i] + v for v in inner]
    picks = [routes[k : k + 1, :] for k in range(2)]
    chosen = []
    for k in range(2):
        value = jnp.zeros_like(total_lp[0])
        for i in range(n_experts):
            value = jnp.where(picks[k] == i, total_lp[i], value)
        chosen.append(value)
    top = jnp.maximum(chosen[0], chosen[1])
    share = [jnp.exp(v - top) for v in chosen]
    inv = 1.0 / (share[0] + share[1])
    share = [v * inv for v in share]
    wts[e] = jnp.zeros(wts.shape[1:], F32)
    for i in range(n_experts):
        wts[e, i : i + 1, :] = jnp.where(picks[0] == i, share[0], 0.0) + jnp.where(
            picks[1] == i, share[1], 0.0
        )
    for k in range(1, n_ep):
        send(wts.at[e], wts.at[e], wts_s.at[k - 1], wts_r.at[k - 1], ((e + k) % n_ep, t))

    slots = psend.shape[0]
    to_partner = {}

    def experts(block, order):
        wrow = wts[block, pl.ds(e, 1), :]
        wcol = jnp.transpose(jnp.broadcast_to(wrow, (LANES, n_tok)))
        wide = 256
        wcol = jnp.concatenate([wcol] * (wide // LANES), axis=1)

        def up(j, carry):
            cols = pl.ds(pl.multiple_of(j * wide, wide), wide)
            g = dot(rows_tok[block], eg[:, cols])
            u = dot(rows_tok[block], eu[:, cols])
            hid[:, cols] = (silu(g) * u * wcol).astype(BF16)
            return carry

        lax.fori_loop(0, ff // wide, up, 0)
        slot = order % slots
        if order >= slots:
            earlier = to_partner[order - slots]
            earlier.wait_send()
            pending[:] = [copy for copy in pending if copy is not earlier]

        def down(k, carry):
            at = pl.ds(pl.multiple_of(k * feats, feats), feats)
            other = pl.ds(pl.multiple_of((CORES * k + 1 - c) * feats, feats), feats)
            own = pl.ds(pl.multiple_of((CORES * k + c) * feats, feats), feats)
            psend[slot, :, at] = dot(hid[...], ed[:, other]).astype(BF16)
            pmine[block, :, at] = dot(hid[...], ed[:, own]).astype(BF16)
            return carry

        lax.fori_loop(0, n_z, down, 0)
        to_partner[order] = send(
            psend.at[slot], precv.at[block], pd_s.at[order], pd_r.at[order], partner
        )

    get_eg.wait()
    get_eu.wait()
    get_ed.wait()
    experts(e, 0)

    lane = lax.broadcasted_iota(jnp.int32, (1, LANES), 1)
    rate = jnp.exp(lograte[...])
    for k in range(nblk):
        at = pl.ds(k * BLOCK, BLOCK)
        v = step[:, at]
        dt = jnp.maximum(v, 0.0) + jnp.log(1.0 + jnp.exp(-jnp.abs(v)))
        cum = extra[:, at] - dt * rate
        hop = 1
        while hop < BLOCK:
            cum = cum + jnp.where(lane >= hop, pltpu.roll(cum, hop, 1), 0.0)
            hop *= 2
        grown = jnp.exp(cum)
        left = jnp.exp(cum[:, BLOCK - 1 :] - cum) * dt
        rows_s[k, 0:heads, :] = cum
        rows_s[k, 8 : 8 + heads, :] = dt
        rows_s[k, 16 : 16 + heads, :] = left
        rows_s[k, 24 : 24 + heads, :] = grown

    def spread(cols, first):
        pieces = []
        for j in range(width // LANES):
            low = cols[:, first + 2 * j : first + 2 * j + 1]
            high = cols[:, first + 2 * j + 1 : first + 2 * j + 2]
            pieces.append(jnp.where(lane < STATE, low, high))
        return jnp.concatenate(pieces, axis=1) if len(pieces) > 1 else pieces[0]

    get_x.wait()
    get_b.wait()
    get_c.wait()

    @pl.when(e > 0)
    def _():
        for copy in halo:
            copy.wait_recv()

    x_w = xtaps[...].astype(F32)
    bc_w = jnp.concatenate([btaps[:, lane_b], ctaps[:, lane_b]], axis=1).astype(F32)
    lane2 = lax.broadcasted_iota(jnp.int32, (1, 2 * LANES), 1) % LANES
    in_group = (lane2 >= within) & (lane2 < within + STATE)
    taps = x_w.shape[0]

    def conv(ref, w, k):
        v = ref[pl.ds(pl.multiple_of(k * BLOCK, BLOCK), BLOCK + HALO), :].astype(F32)
        total = v[HALO:] * w[taps - 1 :]
        for j in range(taps - 1):
            total = total + pltpu.roll(v, taps - 1 - j, 0)[HALO:] * w[j : j + 1]
        return silu(total)

    st_s[...] = jnp.zeros_like(st_s)
    dec_s[...] = jnp.ones_like(dec_s)

    def first_pass(k, carry):
        rows = pl.ds(pl.multiple_of(k * BLOCK, BLOCK), BLOCK)
        xs = conv(xpad, x_w, k).astype(BF16)
        bc = jnp.where(in_group, conv(bcpad, bc_w, k), 0.0).astype(BF16)
        xs_s[rows, :] = xs
        bc_s[rows, :] = bc
        cols = jnp.transpose(rows_s[k])
        xw = (xs.astype(F32) * spread(cols, 16)).astype(BF16)
        block_state = dot(bc[:, :LANES], xw, (((0,), (0,)), ((), ())))
        gone = spread(cols[BLOCK - 8 :, :], 24)[7:8, :]
        prev_s[k] = st_s[...]
        dpre_s[k] = dec_s[...]
        st_s[...] = st_s[...] * gone + block_state
        dec_s[...] = dec_s[...] * gone
        return carry

    lax.fori_loop(0, nblk, first_pass, 0)

    group_rows = pl.ds(pl.multiple_of(within, STATE), STATE)
    smsg[0:STATE, :] = st_s[group_rows, :].astype(BF16)
    smsg[STATE : STATE + 16, :] = jnp.concatenate([dec_s[...]] * 2, axis=0).astype(BF16)
    state_copies = [
        remote(smsg, srecv.at[k], state_s.at[k], state_r.at[k], ((e + 1 + k) % n_ep, t))
        for k in range(n_ep - 1)
    ]
    for k, copy in enumerate(state_copies):
        pl.when(e + 1 + k < n_ep)(copy.start)

    for k in range(1, n_ep):
        src = (e - k + n_ep) % n_ep
        arrived(wts.at[src], wts_r.at[k - 1])
    for d in range(1, half_ring + 1):
        for way in range(2):
            share_tokens(way, d)
        if d == 1:
            for k in range(1, n_z):
                arrived(wk.at[e, (z - k + n_z) % n_z], wz_r.at[k - 1])

            def weight_view(block, way, k, last):
                slab = wk.at[block, (z - k + n_z) % n_z]
                if last:
                    return slab.at[pl.ds(way * (rows_w // 2), rows_w // 2), :]
                return slab

            def send_weight(way, step_d):
                block = at_ring(-(step_d - 1) if way == 0 else step_d - 1)
                for k in range(1, n_z):
                    view = weight_view(block, way, k, step_d == half_ring)
                    send(
                        view,
                        view,
                        wr_s.at[way, step_d - 1, k - 1],
                        wr_r.at[way, step_d - 1, k - 1],
                        toward[way],
                    )

            def weight_arrived(way, step_d):
                block = at_ring(-step_d if way == 0 else step_d)
                for k in range(1, n_z):
                    view = weight_view(block, way, k, step_d == half_ring)
                    arrived(view, wr_r.at[way, step_d - 1, k - 1])

            for way in range(2):
                send_weight(way, 1)
        for way in range(2):
            shared_tokens(way, d)
        if d < half_ring:
            for way in range(2):
                order = 2 * d - 1 + way
                experts(at_ring(-d if way == 0 else d), order)
        else:
            order = 2 * d - 1
            experts(at_ring(d), order)

    def order_of(way, d):
        if d == half_ring:
            return 2 * d - 1
        if d == 0:
            return 0
        return 2 * d - 1 + way

    def partner_sum(block, order):
        arrived(precv.at[block], pd_r.at[order])

    keep = feats * n_z
    keep_half = keep // 2

    def ring_sum(d, way):
        block = at_ring(d if way == 0 else -d)
        if d == half_ring:
            cols = pl.ds(way * keep_half, keep_half)
            value = pmine[block, :, cols].astype(F32) + precv[block, :, cols].astype(F32)
            pmine[block, :, cols] = value.astype(BF16)
            view = pmine.at[block, :, cols]
            send(
                view, rsrecv.at[way, d - 1, :, cols], rs_s.at[way, d - 1], rs_r.at[way, d - 1], toward[way]
            )
            return
        last = d == half_ring - 1
        cols = pl.ds(way * keep_half, keep_half) if last else pl.ds(0, keep)
        arrived(rsrecv.at[way, d, :, cols], rs_r.at[way, d])
        if last:
            rest = pl.ds((1 - way) * keep_half, keep_half)
            pmine[block, :, rest] = (
                pmine[block, :, rest].astype(F32) + precv[block, :, rest].astype(F32)
            ).astype(BF16)
        pmine[block, :, cols] = (
            pmine[block, :, cols].astype(F32)
            + precv[block, :, cols].astype(F32)
            + rsrecv[way, d, :, cols].astype(F32)
        ).astype(BF16)
        send(
            pmine.at[block], rsrecv.at[way, d - 1], rs_s.at[way, d - 1], rs_r.at[way, d - 1], toward[way]
        )

    partner_sum(at_ring(half_ring), order_of(0, half_ring))
    for way in range(2):
        ring_sum(half_ring, way)

    ent[...] = jnp.zeros_like(ent)
    for k in reversed(range(n_ep - 1)):

        @pl.when(e > k)
        def _(k=k):
            arrived(srecv.at[k], state_r.at[k])
            before = ent[group_rows, :]
            gone = srecv[k, STATE : STATE + 16, :].astype(F32)[0:1, :]
            ent[group_rows, :] = before * gone + srecv[k, 0:STATE, :].astype(F32)

    get_gate.wait()
    d_row = dscale[...]
    g_row = gnorm[...].astype(F32)
    row_id = lax.broadcasted_iota(jnp.int32, (BLOCK, BLOCK), 0)
    col_id = lax.broadcasted_iota(jnp.int32, (BLOCK, BLOCK), 1)
    same_head = (
        lax.broadcasted_iota(jnp.int32, (width, width), 0) // STATE
        == lax.broadcasted_iota(jnp.int32, (width, width), 1) // STATE
    )
    mean_of = jnp.where(same_head, 1.0 / STATE, 0.0).astype(BF16)

    def second_pass(k):
        rows = pl.ds(pl.multiple_of(k * BLOCK, BLOCK), BLOCK)
        xs_f = xs_s[rows, :].astype(F32)
        bs = bc_s[rows, pl.ds(0, LANES)]
        cs = bc_s[rows, pl.ds(LANES, LANES)]
        row_q = rows_s[k]
        cols = jnp.transpose(row_q)
        scores = dot(cs, bs, (((1,), (1,)), ((), ())))
        x_dt = (xs_f * spread(cols, 8)).astype(BF16)
        inner = []
        for j in range(width // LANES):
            both = []
            for h in (2 * j, 2 * j + 1):
                diff = cols[:, h : h + 1] - row_q[h : h + 1, :]
                link = jnp.exp(jnp.where(row_id >= col_id, diff, -1e30))
                both.append(dot((scores * link).astype(BF16), x_dt[:, j * LANES : (j + 1) * LANES]))
            inner.append(jnp.where(lane < STATE, both[0], both[1]))
        inner = jnp.concatenate(inner, axis=1) if len(inner) > 1 else inner[0]
        prev = prev_s[k] + ent[...] * dpre_s[k, 0:1, :]
        carried = dot(cs, prev.astype(BF16)) * spread(cols, 24)
        gated = (inner + carried + d_row * xs_f) * silu(gate[rows, :].astype(F32))
        square = gated * gated
        high = square.astype(BF16)
        low = (square - high.astype(F32)).astype(BF16)
        mean = dot(high, mean_of) + dot(low, mean_of)
        mixed[rows, :] = (gated * lax.rsqrt(mean + EPS) * g_row).astype(BF16)

    chip_rows = rows_dev * CORES
    per_chip = chip_rows // BLOCK

    def mix_for(k):
        target = (z + k) % n_z

        def body(i, carry):
            second_pass(target * per_chip + i)
            return carry

        lax.fori_loop(0, per_chip, body, 0)
        view = mixed.at[pl.ds(pl.multiple_of(target * chip_rows, chip_rows), chip_rows), :]
        if k:
            send(view, mrecv.at[z], a2a_s.at[k - 1], a2a_r.at[k - 1], (e, (t + CORES * k) % n_tp))
        else:
            own = pl.ds(pl.multiple_of(z * chip_rows, chip_rows), chip_rows)
            mrecv[z] = mixed[own, :]

    def ring_step(d):
        for way in range(2):
            partner_sum(at_ring(d if way == 0 else -d), order_of(1 - way, d))
            ring_sum(d, way)

    ring_steps = list(range(half_ring - 1, 0, -1))
    weight_steps = list(range(1, half_ring + 1))
    for i, k in enumerate(list(range(1, n_z)) + [0]):
        mix_for(k)
        if i >= n_z // 2 - 1 and ring_steps:
            ring_step(ring_steps.pop(0))
        if i >= n_z // 2 and weight_steps and weight_steps[0] < half_ring:
            d = weight_steps.pop(0)
            for way in range(2):
                weight_arrived(way, d)
                send_weight(way, d + 1)
    for d in ring_steps:
        ring_step(d)

    partner_sum(e, 0)
    for way in range(2):
        arrived(rsrecv.at[way, 0], rs_r.at[way, 0])

    def own_sum(target):
        at = pl.ds(pl.multiple_of(target * feats, feats), feats)
        return (
            pmine[e, :, at].astype(F32)
            + precv[e, :, at].astype(F32)
            + rsrecv[0, 0, :, at].astype(F32)
            + rsrecv[1, 0, :, at].astype(F32)
        )

    for k in range(1, n_z):
        target = (z + k) % n_z
        zsend[k - 1] = own_sum(target).astype(BF16)
        send(zsend.at[k - 1], zrecv.at[k - 1], zs_s.at[k - 1], zs_r.at[k - 1], (e, (t + CORES * k) % n_tp))

    while weight_steps and weight_steps[0] < half_ring:
        d = weight_steps.pop(0)
        for way in range(2):
            weight_arrived(way, d)
            send_weight(way, d + 1)

    for k in range(1, n_z):
        arrived(mrecv.at[(z - k + n_z) % n_z], a2a_r.at[k - 1])
    for copy in get_w:
        copy.wait()

    def project(block, order):
        def rows_of(core):
            return pl.ds(pl.multiple_of(core * rows_dev, rows_dev), rows_dev)

        def product(core):
            total = dot(mrecv[0, rows_of(core), :], wk[block, 0])
            for k in range(1, n_z):
                total = total + dot(mrecv[k, rows_of(core), :], wk[block, k])
            return total

        pjsend[order] = product(1 - c)
        send(pjsend.at[order], pjrecv.at[order], pj_s.at[order], pj_r.at[order], partner)
        pjown[order] = product(c)

    def finish(block, order):
        arrived(pjrecv.at[order], pj_r.at[order])
        cols = pl.ds(pl.multiple_of(block * part, part), part)
        out[:, cols] = (pjown[order] + pjrecv[order]).astype(BF16)

    project(e, 0)
    done = [(e, 0)]
    for d in range(1, half_ring):
        for way in range(2):
            block = at_ring(-d if way == 0 else d)
            project(block, order_of(way, d))
            done.append((block, order_of(way, d)))

    total = own_sum(z)
    for k in range(1, n_z):
        arrived(zrecv.at[k - 1], zs_r.at[k - 1])
        total = total + zrecv[k - 1].astype(F32)
    eout[...] = total.astype(BF16)

    for way in range(2):
        weight_arrived(way, half_ring)
    block = at_ring(half_ring)
    project(block, order_of(0, half_ring))
    done.append((block, order_of(0, half_ring)))
    for block, order in done:
        finish(block, order)

    for copy in pending:
        copy.wait_send()

    @pl.when(e < n_ep - 1)
    def _():
        for copy in halo:
            copy.wait_send()

    for k, copy in enumerate(state_copies):
        pl.when(e + 1 + k < n_ep)(copy.wait_send)


def fused(n_ep, n_tp, args):
    (
        x,
        gate_logits,
        b_map,
        c_map,
        xtaps,
        btaps,
        ctaps,
        step,
        lograte,
        extra,
        dscale,
        gnorm,
        wout,
        tokens,
        pnorm,
        group_cols,
        expert_cols,
        routes,
        eg,
        eu,
        ed,
    ) = args
    n_z = n_tp // CORES
    half_ring = n_ep // 2
    length, width = x.shape
    heads = dscale.shape[0]
    nblk = length // BLOCK
    n_tok, depth = tokens.shape
    feats = depth // n_tp
    ff = eg.shape[2]
    rows_w, cols_w = wout.shape
    part = cols_w // n_ep
    rows_dev = length // n_tp
    chip_rows = rows_dev * CORES
    n_rows = expert_cols.shape[1] + group_cols.shape[1]
    router = jnp.concatenate([expert_cols, group_cols], axis=1).T
    router = jnp.pad(router, ((0, -n_rows % 16), (0, 0)))
    w_rows = -(-expert_cols.shape[1] // 8) * 8
    slots = max(2, min(n_ep, 16 // n_ep))
    keep = n_z * feats
    anywhere = pl.BlockSpec(memory_space=pl.ANY)
    vmem = pl.BlockSpec(memory_space=pltpu.VMEM)
    dma = pltpu.SemaphoreType.DMA
    scratch = [
        pltpu.VMEM((length + HALO, width), BF16),
        pltpu.VMEM((length + HALO, 2 * LANES), BF16),
        pltpu.VMEM((length, width), BF16),
        pltpu.VMEM((depth, ff), BF16),
        pltpu.VMEM((depth, ff), BF16),
        pltpu.VMEM((ff, depth), BF16),
        pltpu.VMEM((n_ep, n_z, rows_w, part), BF16),
        pltpu.VMEM((n_ep, n_tok, depth), BF16),
        pltpu.VMEM((n_ep, w_rows, n_tok), F32),
        pltpu.VMEM((n_tok, ff), BF16),
        pltpu.VMEM((slots, n_tok, keep), BF16),
        pltpu.VMEM((n_ep, n_tok, keep), BF16),
        pltpu.VMEM((n_ep, n_tok, keep), BF16),
        pltpu.VMEM((2, half_ring, n_tok, keep), BF16),
        pltpu.VMEM((n_z - 1, n_tok, feats), BF16),
        pltpu.VMEM((n_z - 1, n_tok, feats), BF16),
        pltpu.VMEM((length, width), BF16),
        pltpu.VMEM((length, 2 * LANES), BF16),
        pltpu.VMEM((nblk, BLOCK, BLOCK), F32),
        pltpu.VMEM((nblk, LANES, width), F32),
        pltpu.VMEM((nblk, 8, width), F32),
        pltpu.VMEM((LANES, width), F32),
        pltpu.VMEM((8, width), F32),
        pltpu.VMEM((STATE + 16, width), BF16),
        pltpu.VMEM((n_ep - 1, STATE + 16, width), BF16),
        pltpu.VMEM((LANES, width), F32),
        pltpu.VMEM((length, width), BF16),
        pltpu.VMEM((n_z, chip_rows, width), BF16),
        pltpu.VMEM((n_ep, rows_dev, part), F32),
        pltpu.VMEM((n_ep, rows_dev, part), F32),
        pltpu.VMEM((n_ep, rows_dev, part), F32),
        dma((8 + n_ep,)),
        dma((3,)),
        dma((3,)),
    ]
    for shape in (
        (2, half_ring),
        (2, half_ring),
        (n_ep - 1,),
        (n_z - 1,),
        (2, half_ring, n_z - 1),
        (n_ep - 1,),
        (n_ep,),
        (2, half_ring),
        (n_z - 1,),
        (n_z - 1,),
        (n_ep,),
    ):
        scratch += [dma(shape), dma(shape)]
    return pl.pallas_call(
        functools.partial(kernel, n_ep, n_tp),
        out_shape=(
            jax.ShapeDtypeStruct((rows_dev, cols_w), BF16),
            jax.ShapeDtypeStruct((n_tok, feats), BF16),
        ),
        in_specs=[anywhere] * 9 + [vmem] * 11,
        out_specs=(vmem, vmem),
        scratch_shapes=scratch,
        name="fused",
        compiler_params=pltpu.CompilerParams(
            collective_id=0, has_side_effects=True, vmem_limit_bytes=67_000_000
        ),
    )(
        x,
        gate_logits,
        b_map,
        c_map,
        wout,
        tokens,
        eg[0],
        eu[0],
        ed[0],
        xtaps,
        btaps,
        ctaps,
        step,
        extra,
        lograte.reshape(heads, 1),
        jnp.repeat(dscale, width // heads).reshape(1, width),
        gnorm.reshape(1, width),
        pnorm.reshape(1, depth),
        router,
        routes.T,
    )


def solution(mesh):
    n_ep, n_tp = mesh.shape["ep"], mesh.shape["tp"]
    in_specs = (
        P("ep", "tp"),
        P("ep", "tp"),
        P("ep", None),
        P("ep", None),
        P(None, "tp"),
        P(),
        P(),
        P("tp", "ep"),
        P("tp"),
        P("tp", "ep"),
        P("tp"),
        P("tp"),
        P("tp", None),
        P("ep", None),
        P(),
        P(),
        P(),
        P("ep", None),
        P("ep", None, "tp"),
        P("ep", None, "tp"),
        P("ep", "tp", None),
    )
    out_specs = (P(("ep", "tp"), None), P("ep", "tp"))
    return jax.shard_map(
        lambda *args: fused(n_ep, n_tp, args),
        mesh=mesh,
        in_specs=in_specs,
        out_specs=out_specs,
        check_vma=False,
    )
```

time: 211 us -> 95 us (0.45)
  the two profiles are of different devices: /device:TPU:0 before, /device:TPU:13 now
where the time goes in v1:
time: 95 us; the launch traced here: 94.6 us
  Pallas kernels  84.4 us (89%)
  local copies, waits for them, and re-layouts  8.86 us (9%)
    pallas_call x1, Pallas kernels, fused(): pl.pallas_call(functools.partial(kernel, n_ep, n_tp), out_shape=(jax.Shap...  84.4 us
    unnamed x4, local copies, waits for them, and re-layouts  3 us

profile of v1, /device:TPU:13, one launch (start us, length us, event | category | flops | bytes accessed | tf_op | source)
XLA Modules:
  0.0 94.6 jit_solution(5343118048201629534)
XLA Ops:
  0.6 1.3 %reshape.14.gnorm = bf16[1,256]{1,0:T(2,128)(2,1)} reshape(bf16[256]{0:T(256)(128)(2,1)} %param.32) | data formatting | bytes 1024 | tf_op jit(solution)/shard_map/reshape | solution.py:808
  1.9 1.3 %copy.23.lograte = f32[4,1]{1,0:T(4,128)} copy(f32[4,1]{0,1:T(1,128)} %bitcast.11) | data formatting | bytes 32 | tf_op jit(solution)/shard_map/reshape | solution.py:806
  3.2 0.7 broadcast_in_dim.3
  3.9 0.7 reshape_reshape.3.dscale
  4.6 1.3 %reshape.15.pnorm = bf16[1,2048]{1,0:T(2,128)(2,1)} reshape(bf16[2048]{0:T(1024)(128)(2,1)} %param.35) | data formatting | bytes 8192 | tf_op jit(solution)/shard_map/reshape | solution.py:809
  5.9 0.8 maximum_bitcast_fusion
  6.6 0.6 pad.4.router
  7.2 84.4 %fused.1 = (bf16[256,2048]{1,0:T(8,128)(2,1)}, bf16[256,256]{1,0:T(8,128)(2,1)}) custom-call(bf16[2048,256]{1,0:T(8,128)(2,1)} %x_hbm.1, bf16[2048,256]{1,0:T(8,128)(2,1)} %gate_hbm.1, bf16[2048,256]{1,0:T(8,128)(2,1)} %b_hbm.1, bf16[2048,256]{1,0:T(8,128)(2,1)} %c_hbm.1, bf16[256,2048]{1,0:T(8,128)(2,1)} %wout_hbm.1, bf16[256,2048]{1,0:T(8,128)(2,1)} %tok_hbm.1, ...), custom_call_target="tpu_custom_call" | custom-call | tf_op jit(solution)/shard_map/fused/pallas_call | solution.py:778
  91.6 0.0 copy-start
  91.6 2.3 %copy.26 = bf16[256,2048]{1,0:T(8,128)(2,1)} copy(bf16[256,2048]{1,0:T(8,128)(2,1)} %get-tuple-element.4) | data formatting | bytes 2097152
  94.0 0.0 copy-done
  94.0 0.7 copy.27
Async XLA Ops:
  91.6 2.4 %copy-start = (bf16[256,256]{1,0:T(8,128)(2,1)S(1)}, bf16[256,256]{1,0:T(8,128)(2,1)}, u32[]{:S(2)}) copy-start(bf16[256,256]{1,0:T(8,128)(2,1)} %get-tuple-element.5) | copy-start | bytes 393220

commit v2 on v1

--- a/solution.py
+++ b/solution.py
@@ -57,7 +57,8 @@
     dscale,
     gnorm,
     pnorm,
-    router,
+    grouter,
+    erouter,
     routes,
     out,
     eout,
@@ -91,7 +92,10 @@
     mrecv,
     pjsend,
     pjown,
+    pjlast,
     pjrecv,
+    result,
+    eresult,
     ld,
     halo_s,
     halo_r,
@@ -127,6 +131,17 @@
     ring = snake(e, n_ep)
     partner = (e, t + 1 - 2 * c)
 
+    def across_z(k):
+        place, bit = 0, 1
+        while bit < n_z:
+            own = z // bit % 2
+            place = place + bit * ((1 - own) if k & bit else own)
+            bit *= 2
+        return place
+
+    def z_device(k):
+        return (e, CORES * across_z(k) + c)
+
     def at_ring(offset):
         return snake((ring + offset + n_ep) % n_ep, n_ep)
 
@@ -146,7 +161,6 @@
     rows_w = wout_hbm.shape[0]
     part = wout_hbm.shape[1] // n_ep
     rows_dev = out.shape[0]
-    n_experts = n_ep
     pending = []
 
     def remote(src, dst, send, recv, device):
@@ -187,15 +201,13 @@
         pl.semaphore_signal(barrier, inc=1, device_id=((e + k) % n_ep, t), device_id_type=MESH)
         peers += 1
     for k in range(1, n_z):
-        pl.semaphore_signal(
-            barrier, inc=1, device_id=(e, (t + CORES * k) % n_tp), device_id_type=MESH
-        )
+        pl.semaphore_signal(barrier, inc=1, device_id=z_device(k), device_id_type=MESH)
         peers += 1
     pl.semaphore_signal(barrier, inc=1, device_id=partner, device_id_type=MESH)
     peers += 1
 
     get_tok.wait()
-    scale = pnorm[...].astype(F32)
+    scale = pnorm[...].astype(F32).reshape(1, depth)
 
     def norm_rows(i, carry):
         rows = pl.ds(pl.multiple_of(i * 32, 32), 32)
@@ -208,31 +220,34 @@
 
     pl.semaphore_wait(barrier, peers)
 
-    def tok_rows(core, way, last):
-        if last:
-            return pl.ds(pl.multiple_of(core * half + way * quarter, quarter), quarter)
-        return pl.ds(pl.multiple_of(core * half, half), half)
-
-    def send_tokens(way, d):
-        block = at_ring(-(d - 1) if way == 0 else d - 1)
-        view = rows_tok.at[block, tok_rows(c, way, d == half_ring), :]
-        send(view, view, tok_s.at[way, d - 1], tok_r.at[way, d - 1], toward[way])
-
-    def share_tokens(way, d):
+    def tok_view(core, way, d, piece):
         block = at_ring(-d if way == 0 else d)
-        view = rows_tok.at[block, tok_rows(c, way, d == half_ring), :]
-        arrived(view, tok_r.at[way, d - 1])
-        if d < half_ring:
-            send_tokens(way, d + 1)
-        send(view, view, tokp_s.at[way, d - 1], tokp_r.at[way, d - 1], partner)
+        if piece == 0:
+            first, count = core * half + way * quarter, quarter
+        else:
+            count = quarter // 2
+            first = core * half + (1 - way) * quarter + (piece - 1) * count
+        return rows_tok.at[block, pl.ds(pl.multiple_of(first, count), count), :]
+
+    def pieces_of(d):
+        return range(1 if d == half_ring else 3)
+
+    def send_tokens(way, d, piece):
+        view = tok_view(c, way, d - 1, piece)
+        send(view, view, tok_s.at[way, d - 1, piece], tok_r.at[way, d - 1, piece], toward[way])
+
+    def share_tokens(d, pieces):
+        for piece in pieces:
+            for way in range(2):
+                view = tok_view(c, way, d, piece)
+                arrived(view, tok_r.at[way, d - 1, piece])
+                if d < half_ring and piece in pieces_of(d + 1):
+                    send_tokens(way, d + 1, piece)
+                send(view, view, tokp_s.at[way, d - 1, piece], tokp_r.at[way, d - 1, piece], partner)
 
     def shared_tokens(way, d):
-        block = at_ring(-d if way == 0 else d)
-        view = rows_tok.at[block, tok_rows(1 - c, way, d == half_ring), :]
-        arrived(view, tokp_r.at[way, d - 1])
-
-    for way in range(2):
-        send_tokens(way, 1)
+        for piece in pieces_of(d):
+            arrived(tok_view(1 - c, way, d, piece), tokp_r.at[way, d - 1, piece])
 
     tail_rows = pl.ds(length - HALO, HALO)
     head_rows = pl.ds(0, HALO)
@@ -257,21 +272,28 @@
         xpad[head_rows, :] = jnp.zeros((HALO, width), BF16)
         bcpad[head_rows, :] = jnp.zeros((HALO, 2 * LANES), BF16)
 
+    for piece in range(2):
+        for way in range(2):
+            send_tokens(way, 1, piece)
+
     mine = pl.ds(pl.multiple_of(e * part, part), part)
-    for k in range(1, n_z):
+    z_order = sorted(range(1, n_z), key=lambda k: (k != 1, -k))
+    for k in z_order:
         send(
             wout_hbm.at[:, mine],
             wk.at[e, z],
             wz_s.at[k - 1],
             wz_r.at[k - 1],
-            (e, (t + CORES * k) % n_tp),
+            z_device(k),
         )
 
-    logits = dot(router[...], rows_tok[e], (((1,), (1,)), ((), ())))
+    n_experts, n_grp = erouter.shape[0], grouter.shape[0]
+    over_rows = (((1,), (1,)), ((), ()))
+    logits = dot(erouter[...], rows_tok[e], over_rows)
     expert_logit = [logits[i : i + 1, :] for i in range(n_experts)]
-    n_grp = max(1, n_experts // 4)
+    logits = dot(grouter[...], rows_tok[e], over_rows)
     per_group = n_experts // n_grp
-    group_logit = [logits[n_experts + i : n_experts + i + 1, :] for i in range(n_grp)]
+    group_logit = [logits[i : i + 1, :] for i in range(n_grp)]
 
     def log_softmax(rows):
         top = functools.reduce(jnp.maximum, rows)
@@ -325,26 +347,24 @@
             earlier.wait_send()
             pending[:] = [copy for copy in pending if copy is not earlier]
 
-        def down(k, carry):
-            at = pl.ds(pl.multiple_of(k * feats, feats), feats)
-            other = pl.ds(pl.multiple_of((CORES * k + 1 - c) * feats, feats), feats)
-            own = pl.ds(pl.multiple_of((CORES * k + c) * feats, feats), feats)
-            psend[slot, :, at] = dot(hid[...], ed[:, other]).astype(BF16)
-            pmine[block, :, at] = dot(hid[...], ed[:, own]).astype(BF16)
-            return carry
-
-        lax.fori_loop(0, n_z, down, 0)
+        def down(into, core):
+            for k in range(n_z):
+                at = pl.ds(k * feats, feats)
+                cols = pl.ds(pl.multiple_of((CORES * k + core) * feats, feats), feats)
+                into[:, at] = dot(hid[...], ed[:, cols]).astype(BF16)
+
+        down(psend.at[slot], 1 - c)
         to_partner[order] = send(
             psend.at[slot], precv.at[block], pd_s.at[order], pd_r.at[order], partner
         )
-
-    get_eg.wait()
-    get_eu.wait()
-    get_ed.wait()
-    experts(e, 0)
+        down(pmine.at[block], c)
 
     lane = lax.broadcasted_iota(jnp.int32, (1, LANES), 1)
-    rate = jnp.exp(lograte[...])
+    head_row = lax.broadcasted_iota(jnp.int32, (heads, 1), 0)
+    rate = jnp.zeros((heads, 1), F32)
+    for h in range(heads):
+        rate = jnp.where(head_row == h, lograte[h], rate)
+    rate = jnp.exp(rate)
     for k in range(nblk):
         at = pl.ds(k * BLOCK, BLOCK)
         v = step[:, at]
@@ -412,6 +432,30 @@
 
     lax.fori_loop(0, nblk, first_pass, 0)
 
+    def weight_view(block, way, k, d):
+        slab = wk.at[block, across_z(k)]
+        if d == half_ring:
+            return slab.at[pl.ds(way * (rows_w // 2), rows_w // 2), :]
+        return slab
+
+    def send_weight(way, d, k):
+        view = weight_view(at_ring(-(d - 1) if way == 0 else d - 1), way, k, d)
+        send(view, view, wr_s.at[way, d - 1, k - 1], wr_r.at[way, d - 1, k - 1], toward[way])
+
+    def first_weight(k):
+        arrived(wk.at[e, across_z(k)], wz_r.at[k - 1])
+        for way in range(2):
+            send_weight(way, 1, k)
+
+    def weight_arrived(way, d, k):
+        view = weight_view(at_ring(-d if way == 0 else d), way, k, d)
+        arrived(view, wr_r.at[way, d - 1, k - 1])
+
+    def pass_weight(d, k):
+        for way in range(2):
+            weight_arrived(way, d, k)
+            send_weight(way, d + 1, k)
+
     group_rows = pl.ds(pl.multiple_of(within, STATE), STATE)
     smsg[0:STATE, :] = st_s[group_rows, :].astype(BF16)
     smsg[STATE : STATE + 16, :] = jnp.concatenate([dec_s[...]] * 2, axis=0).astype(BF16)
@@ -421,52 +465,14 @@
     ]
     for k, copy in enumerate(state_copies):
         pl.when(e + 1 + k < n_ep)(copy.start)
-
-    for k in range(1, n_ep):
-        src = (e - k + n_ep) % n_ep
-        arrived(wts.at[src], wts_r.at[k - 1])
-    for d in range(1, half_ring + 1):
-        for way in range(2):
-            share_tokens(way, d)
-        if d == 1:
-            for k in range(1, n_z):
-                arrived(wk.at[e, (z - k + n_z) % n_z], wz_r.at[k - 1])
-
-            def weight_view(block, way, k, last):
-                slab = wk.at[block, (z - k + n_z) % n_z]
-                if last:
-                    return slab.at[pl.ds(way * (rows_w // 2), rows_w // 2), :]
-                return slab
-
-            def send_weight(way, step_d):
-                block = at_ring(-(step_d - 1) if way == 0 else step_d - 1)
-                for k in range(1, n_z):
-                    view = weight_view(block, way, k, step_d == half_ring)
-                    send(
-                        view,
-                        view,
-                        wr_s.at[way, step_d - 1, k - 1],
-                        wr_r.at[way, step_d - 1, k - 1],
-                        toward[way],
-                    )
-
-            def weight_arrived(way, step_d):
-                block = at_ring(-step_d if way == 0 else step_d)
-                for k in range(1, n_z):
-                    view = weight_view(block, way, k, step_d == half_ring)
-                    arrived(view, wr_r.at[way, step_d - 1, k - 1])
-
-            for way in range(2):
-                send_weight(way, 1)
-        for way in range(2):
-            shared_tokens(way, d)
-        if d < half_ring:
-            for way in range(2):
-                order = 2 * d - 1 + way
-                experts(at_ring(-d if way == 0 else d), order)
-        else:
-            order = 2 * d - 1
-            experts(at_ring(d), order)
+    for way in range(2):
+        send_tokens(way, 1, 2)
+    get_eg.wait()
+    get_eu.wait()
+    get_ed.wait()
+    experts(e, 0)
+    share_tokens(1, [0])
+    share_tokens(1, [1])
 
     def order_of(way, d):
         if d == half_ring:
@@ -509,10 +515,6 @@
             pmine.at[block], rsrecv.at[way, d - 1], rs_s.at[way, d - 1], rs_r.at[way, d - 1], toward[way]
         )
 
-    partner_sum(at_ring(half_ring), order_of(0, half_ring))
-    for way in range(2):
-        ring_sum(half_ring, way)
-
     ent[...] = jnp.zeros_like(ent)
     for k in reversed(range(n_ep - 1)):
 
@@ -524,8 +526,11 @@
             ent[group_rows, :] = before * gone + srecv[k, 0:STATE, :].astype(F32)
 
     get_gate.wait()
-    d_row = dscale[...]
-    g_row = gnorm[...].astype(F32)
+    head_lane = lax.broadcasted_iota(jnp.int32, (1, width), 1) // STATE
+    d_row = jnp.zeros((1, width), F32)
+    for h in range(heads):
+        d_row = jnp.where(head_lane == h, dscale[h], d_row)
+    g_row = gnorm[...].astype(F32).reshape(1, width)
     row_id = lax.broadcasted_iota(jnp.int32, (BLOCK, BLOCK), 0)
     col_id = lax.broadcasted_iota(jnp.int32, (BLOCK, BLOCK), 1)
     same_head = (
@@ -565,7 +570,7 @@
     per_chip = chip_rows // BLOCK
 
     def mix_for(k):
-        target = (z + k) % n_z
+        target = across_z(k)
 
         def body(i, carry):
             second_pass(target * per_chip + i)
@@ -574,7 +579,7 @@
         lax.fori_loop(0, per_chip, body, 0)
         view = mixed.at[pl.ds(pl.multiple_of(target * chip_rows, chip_rows), chip_rows), :]
         if k:
-            send(view, mrecv.at[z], a2a_s.at[k - 1], a2a_r.at[k - 1], (e, (t + CORES * k) % n_tp))
+            send(view, mrecv.at[z], a2a_s.at[k - 1], a2a_r.at[k - 1], z_device(k))
         else:
             own = pl.ds(pl.multiple_of(z * chip_rows, chip_rows), chip_rows)
             mrecv[z] = mixed[own, :]
@@ -584,19 +589,42 @@
             partner_sum(at_ring(d if way == 0 else -d), order_of(1 - way, d))
             ring_sum(d, way)
 
-    ring_steps = list(range(half_ring - 1, 0, -1))
-    weight_steps = list(range(1, half_ring + 1))
-    for i, k in enumerate(list(range(1, n_z)) + [0]):
+    mixes = [k for k in range(2, n_z)] + [1, 0]
+    mix_for(mixes.pop(0))
+    waiting = list(z_order)
+    share_tokens(1, [2])
+    first_weight(waiting.pop(0))
+    for k in range(1, n_ep):
+        arrived(wts.at[(e - k + n_ep) % n_ep], wts_r.at[k - 1])
+    for d in range(1, half_ring + 1):
+        if 1 < d < half_ring:
+            share_tokens(d, pieces_of(d))
+        for way in range(2):
+            shared_tokens(way, d)
+        if d < half_ring:
+            for way in range(2):
+                experts(at_ring(-d if way == 0 else d), order_of(way, d))
+                if way == 0 and d + 1 == half_ring:
+                    share_tokens(half_ring, pieces_of(half_ring))
+        else:
+            experts(at_ring(d), order_of(0, d))
+    partner_sum(at_ring(half_ring), order_of(0, half_ring))
+    for way in range(2):
+        ring_sum(half_ring, way)
+    first_weight(waiting.pop(0))
+    mix_for(mixes.pop(0))
+    for d in range(half_ring - 1, 0, -1):
+        if mixes:
+            mix_for(mixes.pop(0))
+        ring_step(d)
+    while waiting:
+        first_weight(waiting.pop(0))
+    for k in mixes:
         mix_for(k)
-        if i >= n_z // 2 - 1 and ring_steps:
-            ring_step(ring_steps.pop(0))
-        if i >= n_z // 2 and weight_steps and weight_steps[0] < half_ring:
-            d = weight_steps.pop(0)
-            for way in range(2):
-                weight_arrived(way, d)
-                send_weight(way, d + 1)
-    for d in ring_steps:
-        ring_step(d)
+
+    for d in range(1, half_ring):
+        for k in z_order[:-1]:
+            pass_weight(d, k)
 
     partner_sum(e, 0)
     for way in range(2):
@@ -612,39 +640,64 @@
         )
 
     for k in range(1, n_z):
-        target = (z + k) % n_z
+        target = across_z(k)
         zsend[k - 1] = own_sum(target).astype(BF16)
-        send(zsend.at[k - 1], zrecv.at[k - 1], zs_s.at[k - 1], zs_r.at[k - 1], (e, (t + CORES * k) % n_tp))
-
-    while weight_steps and weight_steps[0] < half_ring:
-        d = weight_steps.pop(0)
-        for way in range(2):
-            weight_arrived(way, d)
-            send_weight(way, d + 1)
+        send(zsend.at[k - 1], zrecv.at[k - 1], zs_s.at[k - 1], zs_r.at[k - 1], z_device(k))
+
+    for d in range(1, half_ring):
+        pass_weight(d, z_order[-1])
 
     for k in range(1, n_z):
-        arrived(mrecv.at[(z - k + n_z) % n_z], a2a_r.at[k - 1])
+        arrived(mrecv.at[across_z(k)], a2a_r.at[k - 1])
     for copy in get_w:
         copy.wait()
 
+    def rows_of(core):
+        return pl.ds(pl.multiple_of(core * rows_dev, rows_dev), rows_dev)
+
+    def product(core, block):
+        total = dot(mrecv[0, rows_of(core), :], wk[block, 0])
+        for k in range(1, n_z):
+            total = total + dot(mrecv[k, rows_of(core), :], wk[block, k])
+        return total
+
+    def give(order):
+        send(pjsend.at[order], pjrecv.at[order], pj_s.at[order], pj_r.at[order], partner)
+
     def project(block, order):
-        def rows_of(core):
-            return pl.ds(pl.multiple_of(core * rows_dev, rows_dev), rows_dev)
-
-        def product(core):
-            total = dot(mrecv[0, rows_of(core), :], wk[block, 0])
-            for k in range(1, n_z):
-                total = total + dot(mrecv[k, rows_of(core), :], wk[block, k])
-            return total
-
-        pjsend[order] = product(1 - c)
-        send(pjsend.at[order], pjrecv.at[order], pj_s.at[order], pj_r.at[order], partner)
-        pjown[order] = product(c)
+        pjsend[order] = product(1 - c, block).astype(BF16)
+        give(order)
+        pjown[order] = product(c, block)
+
+    def project_late(block, order):
+        both = (c, 1 - c)
+        for core, total in zip(both, (pjown.at[order], pjlast)):
+            total[...] = dot(mrecv[z, rows_of(core), :], wk[block, z])
+        for k in z_order:
+            for way in range(2):
+                weight_arrived(way, half_ring, k)
+            place = across_z(k)
+            if k == z_order[-1]:
+                total = pjlast[...] + dot(mrecv[place, rows_of(1 - c), :], wk[block, place])
+                pjsend[order] = total.astype(BF16)
+                give(order)
+                pjown[order] += dot(mrecv[place, rows_of(c), :], wk[block, place])
+            else:
+                for core, total in zip(both, (pjown.at[order], pjlast)):
+                    total[...] += dot(mrecv[place, rows_of(core), :], wk[block, place])
+
+    puts = []
+
+    def put(src, dst, index):
+        copy = pltpu.make_async_copy(src, dst, ld.at[index])
+        copy.start()
+        puts.append(copy)
 
     def finish(block, order):
         arrived(pjrecv.at[order], pj_r.at[order])
+        result[order] = (pjown[order] + pjrecv[order].astype(F32)).astype(BF16)
         cols = pl.ds(pl.multiple_of(block * part, part), part)
-        out[:, cols] = (pjown[order] + pjrecv[order]).astype(BF16)
+        put(result.at[order], out.at[:, cols], order)
 
     project(e, 0)
     done = [(e, 0)]
@@ -658,18 +711,18 @@
     for k in range(1, n_z):
         arrived(zrecv.at[k - 1], zs_r.at[k - 1])
         total = total + zrecv[k - 1].astype(F32)
-    eout[...] = total.astype(BF16)
-
-    for way in range(2):
-        weight_arrived(way, half_ring)
-    block = at_ring(half_ring)
-    project(block, order_of(0, half_ring))
-    done.append((block, order_of(0, half_ring)))
+    eresult[...] = total.astype(BF16)
+    put(eresult, eout, n_ep)
+
     for block, order in done:
         finish(block, order)
+    project_late(at_ring(half_ring), order_of(0, half_ring))
+    finish(at_ring(half_ring), order_of(0, half_ring))
 
     for copy in pending:
         copy.wait_send()
+    for copy in puts:
+        copy.wait()
 
     @pl.when(e < n_ep - 1)
     def _():
@@ -678,6 +731,38 @@
 
     for k, copy in enumerate(state_copies):
         pl.when(e + 1 + k < n_ep)(copy.wait_send)
+
+
+def hand_over_kernel(chunks, a_in, b_in, a_out, b_out, a, b, sems):
+    rows = a.shape[0] // chunks
+    moves = [(a_in.at[pl.ds(i * rows, rows)], a.at[pl.ds(i * rows, rows)], a_out.at[pl.ds(i * rows, rows)]) for i in range(chunks)]
+    moves.append((b_in, b, b_out))
+    reads = [pltpu.make_async_copy(m[0], m[1], sems.at[0, i]) for i, m in enumerate(moves)]
+    writes = [pltpu.make_async_copy(m[1], m[2], sems.at[1, i]) for i, m in enumerate(moves)]
+    for copy in reads:
+        copy.start()
+    for read, write in zip(reads, writes):
+        read.wait()
+        write.start()
+    for copy in writes:
+        copy.wait()
+
+
+def hand_over(a, b):
+    chunks = 4
+    anywhere = pl.BlockSpec(memory_space=pl.ANY)
+    return pl.pallas_call(
+        functools.partial(hand_over_kernel, chunks),
+        out_shape=(jax.ShapeDtypeStruct(a.shape, a.dtype), jax.ShapeDtypeStruct(b.shape, b.dtype)),
+        in_specs=[anywhere] * 2,
+        out_specs=(anywhere, anywhere),
+        scratch_shapes=[
+            pltpu.VMEM(a.shape, a.dtype),
+            pltpu.VMEM(b.shape, b.dtype),
+            pltpu.SemaphoreType.DMA((2, chunks + 1)),
+        ],
+        name="hand_over",
+    )(a, b)
 
 
 def fused(n_ep, n_tp, args):
@@ -716,14 +801,12 @@
     part = cols_w // n_ep
     rows_dev = length // n_tp
     chip_rows = rows_dev * CORES
-    n_rows = expert_cols.shape[1] + group_cols.shape[1]
-    router = jnp.concatenate([expert_cols, group_cols], axis=1).T
-    router = jnp.pad(router, ((0, -n_rows % 16), (0, 0)))
     w_rows = -(-expert_cols.shape[1] // 8) * 8
     slots = max(2, min(n_ep, 16 // n_ep))
     keep = n_z * feats
     anywhere = pl.BlockSpec(memory_space=pl.ANY)
     vmem = pl.BlockSpec(memory_space=pltpu.VMEM)
+    smem = pl.BlockSpec(memory_space=pltpu.SMEM)
     dma = pltpu.SemaphoreType.DMA
     scratch = [
         pltpu.VMEM((length + HALO, width), BF16),
@@ -754,16 +837,19 @@
         pltpu.VMEM((LANES, width), F32),
         pltpu.VMEM((length, width), BF16),
         pltpu.VMEM((n_z, chip_rows, width), BF16),
+        pltpu.VMEM((n_ep, rows_dev, part), BF16),
         pltpu.VMEM((n_ep, rows_dev, part), F32),
-        pltpu.VMEM((n_ep, rows_dev, part), F32),
-        pltpu.VMEM((n_ep, rows_dev, part), F32),
+        pltpu.VMEM((rows_dev, part), F32),
+        pltpu.VMEM((n_ep, rows_dev, part), BF16),
+        pltpu.VMEM((n_ep, rows_dev, part), BF16),
+        pltpu.VMEM((n_tok, feats), BF16),
         dma((8 + n_ep,)),
         dma((3,)),
         dma((3,)),
     ]
     for shape in (
-        (2, half_ring),
-        (2, half_ring),
+        (2, half_ring, 3),
+        (2, half_ring, 3),
         (n_ep - 1,),
         (n_z - 1,),
         (2, half_ring, n_z - 1),
@@ -775,14 +861,14 @@
         (n_ep,),
     ):
         scratch += [dma(shape), dma(shape)]
-    return pl.pallas_call(
+    mixer_out, experts_out = pl.pallas_call(
         functools.partial(kernel, n_ep, n_tp),
         out_shape=(
             jax.ShapeDtypeStruct((rows_dev, cols_w), BF16),
             jax.ShapeDtypeStruct((n_tok, feats), BF16),
         ),
-        in_specs=[anywhere] * 9 + [vmem] * 11,
-        out_specs=(vmem, vmem),
+        in_specs=[anywhere] * 9 + [vmem] * 5 + [smem] * 2 + [vmem] * 5,
+        out_specs=(anywhere, anywhere),
         scratch_shapes=scratch,
         name="fused",
         compiler_params=pltpu.CompilerParams(
@@ -803,13 +889,15 @@
         ctaps,
         step,
         extra,
-        lograte.reshape(heads, 1),
-        jnp.repeat(dscale, width // heads).reshape(1, width),
-        gnorm.reshape(1, width),
-        pnorm.reshape(1, depth),
-        router,
+        lograte,
+        dscale,
+        gnorm,
+        pnorm,
+        group_cols.T,
+        expert_cols.T,
         routes.T,
     )
+    return hand_over(mixer_out, experts_out)
 
 
 def solution(mesh):

time: 95 us -> 78.6 us (0.83)
  the two profiles are of different devices: /device:TPU:13 before, /device:TPU:0 now
where the time goes in v2:
time: 78.6 us; the launch traced here: 78.4 us
  Pallas kernels  77.8 us (99%)
    pallas_call x1, Pallas kernels, fused(): pl.pallas_call(functools.partial(kernel, n_ep, n_tp), out_shape=(jax.Shap...  75.7 us
    pallas_call x1, Pallas kernels, hand_over(): pl.pallas_call(functools.partial(hand_over_kernel, chunks), out_shape=(ja...  2.04 us

profile of v2, /device:TPU:0, one launch (start us, length us, event | category | flops | bytes accessed | tf_op | source)
XLA Modules:
  0.0 78.4 jit_solution(7625096550947076325)
XLA Ops:
  0.6 75.7 %fused.1 = (bf16[256,2048]{1,0:T(8,128)(2,1)}, bf16[256,256]{1,0:T(8,128)(2,1)}) custom-call(bf16[2048,256]{1,0:T(8,128)(2,1)} %x_hbm.1, bf16[2048,256]{1,0:T(8,128)(2,1)} %gate_hbm.1, bf16[2048,256]{1,0:T(8,128)(2,1)} %b_hbm.1, bf16[2048,256]{1,0:T(8,128)(2,1)} %c_hbm.1, bf16[256,2048]{1,0:T(8,128)(2,1)} %wout_hbm.1, bf16[256,2048]{1,0:T(8,128)(2,1)} %tok_hbm.1, ...), custom_call_target="tpu_custom_call" | custom-call | tf_op jit(solution)/shard_map/fused/pallas_call | solution.py:864
  76.4 2.0 %hand_over.1 = (bf16[256,2048]{1,0:T(8,128)(2,1)}, bf16[256,256]{1,0:T(8,128)(2,1)}) custom-call(bf16[256,2048]{1,0:T(8,128)(2,1)} %get-tuple-element.4.a_in, bf16[256,256]{1,0:T(8,128)(2,1)} %get-tuple-element.5.b_in), custom_call_target="tpu_custom_call" | custom-call | tf_op jit(solution)/shard_map/hand_over/pallas_call | solution.py:754

commit v3 on v2

--- a/solution.py
+++ b/solution.py
@@ -48,6 +48,20 @@
     eg_hbm,
     eu_hbm,
     ed_hbm,
+    xtaps_hbm,
+    btaps_hbm,
+    ctaps_hbm,
+    step_hbm,
+    extra_hbm,
+    lograte_hbm,
+    dscale_hbm,
+    gnorm_hbm,
+    pnorm_hbm,
+    grouter_hbm,
+    erouter_hbm,
+    routes_hbm,
+    out,
+    eout,
     xtaps,
     btaps,
     ctaps,
@@ -60,8 +74,6 @@
     grouter,
     erouter,
     routes,
-    out,
-    eout,
     xpad,
     bcpad,
     gate,
@@ -96,6 +108,7 @@
     pjrecv,
     result,
     eresult,
+    eown,
     ld,
     halo_s,
     halo_r,
@@ -109,12 +122,16 @@
     wz_r,
     wr_s,
     wr_r,
+    wx_s,
+    wx_r,
     state_s,
     state_r,
     pd_s,
     pd_r,
     rs_s,
     rs_r,
+    rsl_s,
+    rsl_r,
     zs_s,
     zs_r,
     a2a_s,
@@ -182,8 +199,15 @@
         copy.start()
         return copy
 
-    get_tok = local(tok_hbm, rows_tok.at[e], 0)
-    get_eg = local(eg_hbm, eg, 1)
+    get_tok = [
+        local(tok_hbm.at[rows], rows_tok.at[e, rows], i)
+        for i, rows in enumerate(
+            pl.ds(pl.multiple_of(core * (tok_hbm.shape[0] // CORES), 32), tok_hbm.shape[0] // CORES)
+            for core in (c, 1 - c)
+        )
+    ]
+    get_pnorm = local(pnorm_hbm, pnorm, 19 + n_ep)
+    get_eg = local(eg_hbm, eg, 20 + n_ep)
     get_eu = local(eu_hbm, eu, 2)
     get_ed = local(ed_hbm, ed, 3)
     lane_b = pl.ds(pl.multiple_of(pair * LANES, LANES), LANES)
@@ -195,6 +219,25 @@
         local(wout_hbm.at[:, pl.ds(q * part, part)], wk.at[q, z], 8 + q) for q in range(n_ep)
     ]
 
+    get_small = [
+        local(src, dst, 8 + n_ep + i)
+        for i, (src, dst) in enumerate(
+            (
+                (grouter_hbm, grouter),
+                (erouter_hbm, erouter),
+                (routes_hbm, routes),
+                (step_hbm, step),
+                (extra_hbm, extra),
+                (lograte_hbm, lograte),
+                (xtaps_hbm, xtaps),
+                (btaps_hbm, btaps),
+                (ctaps_hbm, ctaps),
+                (dscale_hbm, dscale),
+                (gnorm_hbm, gnorm),
+            )
+        )
+    ]
+
     barrier = pltpu.get_barrier_semaphore()
     peers = 0
     for k in range(1, n_ep):
@@ -206,7 +249,8 @@
     pl.semaphore_signal(barrier, inc=1, device_id=partner, device_id_type=MESH)
     peers += 1
 
-    get_tok.wait()
+    get_pnorm.wait()
+    get_tok[0].wait()
     scale = pnorm[...].astype(F32).reshape(1, depth)
 
     def norm_rows(i, carry):
@@ -216,7 +260,8 @@
         rows_tok[e, rows, :] = v.astype(BF16)
         return carry
 
-    lax.fori_loop(0, n_tok // 32, norm_rows, 0)
+    steps = half // 32
+    lax.fori_loop(c * steps, c * steps + steps, norm_rows, 0)
 
     pl.semaphore_wait(barrier, peers)
 
@@ -272,20 +317,27 @@
         xpad[head_rows, :] = jnp.zeros((HALO, width), BF16)
         bcpad[head_rows, :] = jnp.zeros((HALO, 2 * LANES), BF16)
 
-    for piece in range(2):
+    for piece in pieces_of(1):
         for way in range(2):
             send_tokens(way, 1, piece)
 
     mine = pl.ds(pl.multiple_of(e * part, part), part)
     z_order = sorted(range(1, n_z), key=lambda k: (k != 1, -k))
-    for k in z_order:
-        send(
-            wout_hbm.at[:, mine],
-            wk.at[e, z],
-            wz_s.at[k - 1],
-            wz_r.at[k - 1],
-            z_device(k),
-        )
+
+    def weight_along_z(k):
+        send(wout_hbm.at[:, mine], wk.at[e, z], wz_s.at[k - 1], wz_r.at[k - 1], z_device(k))
+
+    for k in z_order[:-1]:
+        weight_along_z(k)
+
+    get_tok[1].wait()
+    for copy in get_small:
+        copy.wait()
+    lax.fori_loop((1 - c) * steps, (1 - c) * steps + steps, norm_rows, 0)
+
+    for way in range(2):
+        rest = pl.ds((1 - way) * (n_z * feats // 2), n_z * feats // 2)
+        rsrecv[way, half_ring - 1, :, rest] = jnp.zeros((n_tok, n_z * feats // 2), BF16)
 
     n_experts, n_grp = erouter.shape[0], grouter.shape[0]
     over_rows = (((1,), (1,)), ((), ()))
@@ -432,15 +484,21 @@
 
     lax.fori_loop(0, nblk, first_pass, 0)
 
+    half_w = rows_w // 2
+
     def weight_view(block, way, k, d):
         slab = wk.at[block, across_z(k)]
         if d == half_ring:
-            return slab.at[pl.ds(way * (rows_w // 2), rows_w // 2), :]
-        return slab
+            return slab.at[pl.ds(way * half_w, half_w), :]
+        return slab.at[pl.ds(0, half_w), :] if k == 1 else slab
+
+    def on_ring(d, k):
+        return k != 1 or d < half_ring
 
     def send_weight(way, d, k):
-        view = weight_view(at_ring(-(d - 1) if way == 0 else d - 1), way, k, d)
-        send(view, view, wr_s.at[way, d - 1, k - 1], wr_r.at[way, d - 1, k - 1], toward[way])
+        if on_ring(d, k):
+            view = weight_view(at_ring(-(d - 1) if way == 0 else d - 1), way, k, d)
+            send(view, view, wr_s.at[way, d - 1, k - 1], wr_r.at[way, d - 1, k - 1], toward[way])
 
     def first_weight(k):
         arrived(wk.at[e, across_z(k)], wz_r.at[k - 1])
@@ -448,13 +506,30 @@
             send_weight(way, 1, k)
 
     def weight_arrived(way, d, k):
-        view = weight_view(at_ring(-d if way == 0 else d), way, k, d)
-        arrived(view, wr_r.at[way, d - 1, k - 1])
+        if on_ring(d, k):
+            view = weight_view(at_ring(-d if way == 0 else d), way, k, d)
+            arrived(view, wr_r.at[way, d - 1, k - 1])
 
     def pass_weight(d, k):
         for way in range(2):
             weight_arrived(way, d, k)
             send_weight(way, d + 1, k)
+
+    def direct_rows(d):
+        return pl.ds(0, rows_w) if d == half_ring else pl.ds(half_w, rows_w - half_w)
+
+    def direct_weight(block, order, d):
+        cols = pl.ds(pl.multiple_of(block * part, part), part)
+        send(
+            wout_hbm.at[direct_rows(d), cols],
+            wk.at[block, z, direct_rows(d), :],
+            wx_s.at[order - 1],
+            wx_r.at[order - 1],
+            z_device(1),
+        )
+
+    def direct_arrived(block, order, d):
+        arrived(wk.at[block, across_z(1), direct_rows(d), :], wx_r.at[order - 1])
 
     group_rows = pl.ds(pl.multiple_of(within, STATE), STATE)
     smsg[0:STATE, :] = st_s[group_rows, :].astype(BF16)
@@ -465,13 +540,12 @@
     ]
     for k, copy in enumerate(state_copies):
         pl.when(e + 1 + k < n_ep)(copy.start)
-    for way in range(2):
-        send_tokens(way, 1, 2)
     get_eg.wait()
     get_eu.wait()
     get_ed.wait()
+    weight_along_z(z_order[-1])
+    share_tokens(1, [0])
     experts(e, 0)
-    share_tokens(1, [0])
     share_tokens(1, [1])
 
     def order_of(way, d):
@@ -501,19 +575,23 @@
         last = d == half_ring - 1
         cols = pl.ds(way * keep_half, keep_half) if last else pl.ds(0, keep)
         arrived(rsrecv.at[way, d, :, cols], rs_r.at[way, d])
-        if last:
-            rest = pl.ds((1 - way) * keep_half, keep_half)
-            pmine[block, :, rest] = (
-                pmine[block, :, rest].astype(F32) + precv[block, :, rest].astype(F32)
+        for k in reversed(range(n_z)):
+            at = chunk_of(k)
+            pmine[block, :, at] = (
+                pmine[block, :, at].astype(F32)
+                + precv[block, :, at].astype(F32)
+                + rsrecv[way, d, :, at].astype(F32)
             ).astype(BF16)
-        pmine[block, :, cols] = (
-            pmine[block, :, cols].astype(F32)
-            + precv[block, :, cols].astype(F32)
-            + rsrecv[way, d, :, cols].astype(F32)
-        ).astype(BF16)
-        send(
-            pmine.at[block], rsrecv.at[way, d - 1], rs_s.at[way, d - 1], rs_r.at[way, d - 1], toward[way]
-        )
+            if d == 1:
+                view = rsrecv.at[way, 0, :, at]
+                send(pmine.at[block, :, at], view, rsl_s.at[way, k], rsl_r.at[way, k], toward[way])
+        if d > 1:
+            send(
+                pmine.at[block], rsrecv.at[way, d - 1], rs_s.at[way, d - 1], rs_r.at[way, d - 1], toward[way]
+            )
+
+    def chunk_of(k):
+        return pl.ds(pl.multiple_of(across_z(k) * feats, feats), feats)
 
     ent[...] = jnp.zeros_like(ent)
     for k in reversed(range(n_ep - 1)):
@@ -590,48 +668,46 @@
             ring_sum(d, way)
 
     mixes = [k for k in range(2, n_z)] + [1, 0]
+    waiting = list(z_order)
     mix_for(mixes.pop(0))
-    waiting = list(z_order)
     share_tokens(1, [2])
     first_weight(waiting.pop(0))
+    first_weight(waiting.pop(0))
+    for d in range(1, half_ring):
+        for way in range(2):
+            direct_weight(at_ring(-d if way == 0 else d), order_of(way, d), d)
+    direct_weight(at_ring(half_ring), order_of(0, half_ring), half_ring)
     for k in range(1, n_ep):
         arrived(wts.at[(e - k + n_ep) % n_ep], wts_r.at[k - 1])
-    for d in range(1, half_ring + 1):
-        if 1 < d < half_ring:
-            share_tokens(d, pieces_of(d))
+    for way in range(2):
+        shared_tokens(way, 1)
+    for d in range(1, half_ring):
         for way in range(2):
-            shared_tokens(way, d)
-        if d < half_ring:
-            for way in range(2):
-                experts(at_ring(-d if way == 0 else d), order_of(way, d))
-                if way == 0 and d + 1 == half_ring:
-                    share_tokens(half_ring, pieces_of(half_ring))
-        else:
-            experts(at_ring(d), order_of(0, d))
+            experts(at_ring(-d if way == 0 else d), order_of(way, d))
+            if way == 0:
+                share_tokens(d + 1, pieces_of(d + 1))
+        for way in range(2):
+            shared_tokens(way, d + 1)
+    experts(at_ring(half_ring), order_of(0, half_ring))
     partner_sum(at_ring(half_ring), order_of(0, half_ring))
     for way in range(2):
         ring_sum(half_ring, way)
-    first_weight(waiting.pop(0))
     mix_for(mixes.pop(0))
-    for d in range(half_ring - 1, 0, -1):
-        if mixes:
-            mix_for(mixes.pop(0))
-        ring_step(d)
     while waiting:
         first_weight(waiting.pop(0))
     for k in mixes:
         mix_for(k)
+    for d in range(half_ring - 1, 0, -1):
+        ring_step(d)
 
     for d in range(1, half_ring):
-        for k in z_order[:-1]:
+        for k in z_order:
             pass_weight(d, k)
 
-    partner_sum(e, 0)
-    for way in range(2):
-        arrived(rsrecv.at[way, 0], rs_r.at[way, 0])
-
-    def own_sum(target):
-        at = pl.ds(pl.multiple_of(target * feats, feats), feats)
+    def own_sum(k):
+        at = chunk_of(k)
+        for way in range(2):
+            arrived(rsrecv.at[way, 0, :, at], rsl_r.at[way, k])
         return (
             pmine[e, :, at].astype(F32)
             + precv[e, :, at].astype(F32)
@@ -639,13 +715,11 @@
             + rsrecv[1, 0, :, at].astype(F32)
         )
 
-    for k in range(1, n_z):
-        target = across_z(k)
-        zsend[k - 1] = own_sum(target).astype(BF16)
+    partner_sum(e, 0)
+    for k in reversed(range(1, n_z)):
+        zsend[k - 1] = own_sum(k).astype(BF16)
         send(zsend.at[k - 1], zrecv.at[k - 1], zs_s.at[k - 1], zs_r.at[k - 1], z_device(k))
-
-    for d in range(1, half_ring):
-        pass_weight(d, z_order[-1])
+    eown[...] = own_sum(0)
 
     for k in range(1, n_z):
         arrived(mrecv.at[across_z(k)], a2a_r.at[k - 1])
@@ -676,6 +750,8 @@
         for k in z_order:
             for way in range(2):
                 weight_arrived(way, half_ring, k)
+            if k == 1:
+                direct_arrived(block, order, half_ring)
             place = across_z(k)
             if k == z_order[-1]:
                 total = pjlast[...] + dot(mrecv[place, rows_of(1 - c), :], wk[block, place])
@@ -704,10 +780,11 @@
     for d in range(1, half_ring):
         for way in range(2):
             block = at_ring(-d if way == 0 else d)
+            direct_arrived(block, order_of(way, d), d)
             project(block, order_of(way, d))
             done.append((block, order_of(way, d)))
 
-    total = own_sum(z)
+    total = eown[...]
     for k in range(1, n_z):
         arrived(zrecv.at[k - 1], zs_r.at[k - 1])
         total = total + zrecv[k - 1].astype(F32)
@@ -749,7 +826,7 @@
 
 
 def hand_over(a, b):
-    chunks = 4
+    chunks = 8
     anywhere = pl.BlockSpec(memory_space=pl.ANY)
     return pl.pallas_call(
         functools.partial(hand_over_kernel, chunks),
@@ -789,6 +866,29 @@
         eu,
         ed,
     ) = args
+    operands = (
+        x,
+        gate_logits,
+        b_map,
+        c_map,
+        wout,
+        tokens,
+        eg[0],
+        eu[0],
+        ed[0],
+        xtaps,
+        btaps,
+        ctaps,
+        step,
+        extra,
+        lograte,
+        dscale,
+        gnorm,
+        pnorm,
+        group_cols.T,
+        expert_cols.T,
+        routes.T,
+    )
     n_z = n_tp // CORES
     half_ring = n_ep // 2
     length, width = x.shape
@@ -805,10 +905,12 @@
     slots = max(2, min(n_ep, 16 // n_ep))
     keep = n_z * feats
     anywhere = pl.BlockSpec(memory_space=pl.ANY)
-    vmem = pl.BlockSpec(memory_space=pltpu.VMEM)
-    smem = pl.BlockSpec(memory_space=pltpu.SMEM)
     dma = pltpu.SemaphoreType.DMA
     scratch = [
+        (pltpu.SMEM if v.dtype == F32 and v.ndim == 1 else pltpu.VMEM)(v.shape, v.dtype)
+        for v in operands[9:]
+    ]
+    scratch += [
         pltpu.VMEM((length + HALO, width), BF16),
         pltpu.VMEM((length + HALO, 2 * LANES), BF16),
         pltpu.VMEM((length, width), BF16),
@@ -843,7 +945,8 @@
         pltpu.VMEM((n_ep, rows_dev, part), BF16),
         pltpu.VMEM((n_ep, rows_dev, part), BF16),
         pltpu.VMEM((n_tok, feats), BF16),
-        dma((8 + n_ep,)),
+        pltpu.VMEM((n_tok, feats), F32),
+        dma((21 + n_ep,)),
         dma((3,)),
         dma((3,)),
     ]
@@ -854,8 +957,10 @@
         (n_z - 1,),
         (2, half_ring, n_z - 1),
         (n_ep - 1,),
+        (n_ep - 1,),
         (n_ep,),
         (2, half_ring),
+        (2, n_z),
         (n_z - 1,),
         (n_z - 1,),
         (n_ep,),
@@ -867,36 +972,14 @@
             jax.ShapeDtypeStruct((rows_dev, cols_w), BF16),
             jax.ShapeDtypeStruct((n_tok, feats), BF16),
         ),
-        in_specs=[anywhere] * 9 + [vmem] * 5 + [smem] * 2 + [vmem] * 5,
+        in_specs=[anywhere] * len(operands),
         out_specs=(anywhere, anywhere),
         scratch_shapes=scratch,
         name="fused",
         compiler_params=pltpu.CompilerParams(
             collective_id=0, has_side_effects=True, vmem_limit_bytes=67_000_000
         ),
-    )(
-        x,
-        gate_logits,
-        b_map,
-        c_map,
-        wout,
-        tokens,
-        eg[0],
-        eu[0],
-        ed[0],
-        xtaps,
-        btaps,
-        ctaps,
-        step,
-        extra,
-        lograte,
-        dscale,
-        gnorm,
-        pnorm,
-        group_cols.T,
-        expert_cols.T,
-        routes.T,
-    )
+    )(*operands)
     return hand_over(mixer_out, experts_out)
 
 

time: 78.6 us -> 72.3 us (0.920)
  Pallas kernels: 77.8 us -> 71.1 us
    pallas_call x1, Pallas kernels: 75.7 us -> 68.9 us  [fused(): pl.pallas_call(functools.partial(kernel, n_ep, n_tp), out_shape=(jax.Shap...]
where the time goes in v3:
time: 72.3 us; the launch traced here: 71.9 us
  Pallas kernels  71.1 us (98%)
  between operations  0.81 us (1%)
    pallas_call x1, Pallas kernels, fused(): pl.pallas_call(functools.partial(kernel, n_ep, n_tp), out_shape=(jax.Shap...  68.9 us
    pallas_call x1, Pallas kernels, hand_over(): pl.pallas_call(functools.partial(hand_over_kernel, chunks), out_shape=(ja...  2.15 us

profile of v3, /device:TPU:0, one launch (start us, length us, event | category | flops | bytes accessed | tf_op | source)
XLA Modules:
  0.0 71.9 jit_solution(9109081406554145344)
XLA Ops:
  0.6 68.9 %fused.1 = (bf16[256,2048]{1,0:T(8,128)(2,1)}, bf16[256,256]{1,0:T(8,128)(2,1)}) custom-call(bf16[2048,256]{1,0:T(8,128)(2,1)} %x_hbm.1, bf16[2048,256]{1,0:T(8,128)(2,1)} %gate_hbm.1, bf16[2048,256]{1,0:T(8,128)(2,1)} %b_hbm.1, bf16[2048,256]{1,0:T(8,128)(2,1)} %c_hbm.1, bf16[256,2048]{1,0:T(8,128)(2,1)} %wout_hbm.1, bf16[256,2048]{1,0:T(8,128)(2,1)} %tok_hbm.1, ...), custom_call_target="tpu_custom_call" | custom-call | tf_op jit(solution)/shard_map/fused/pallas_call | solution.py:969
  69.6 2.1 %hand_over.1 = (bf16[256,2048]{1,0:T(8,128)(2,1)}, bf16[256,256]{1,0:T(8,128)(2,1)}) custom-call(bf16[256,2048]{1,0:T(8,128)(2,1)} %get-tuple-element.4.a_in, bf16[256,256]{1,0:T(8,128)(2,1)} %get-tuple-element.5.b_in), custom_call_target="tpu_custom_call" | custom-call | tf_op jit(solution)/shard_map/hand_over/pallas_call | solution.py:831

commit v4 on v3

--- a/solution.py
+++ b/solution.py
@@ -106,37 +106,23 @@
     pjown,
     pjlast,
     pjrecv,
-    result,
-    eresult,
     eown,
-    ld,
+    pool,
     halo_s,
     halo_r,
-    tok_s,
-    tok_r,
-    tokp_s,
-    tokp_r,
-    wts_s,
-    wts_r,
-    wz_s,
-    wz_r,
-    wr_s,
-    wr_r,
-    wx_s,
-    wx_r,
     state_s,
     state_r,
-    pd_s,
+    tok_r,
+    tokp_r,
+    wts_r,
+    wz_r,
+    wr_r,
+    wx_r,
     pd_r,
-    rs_s,
     rs_r,
-    rsl_s,
     rsl_r,
-    zs_s,
     zs_r,
-    a2a_s,
     a2a_r,
-    pj_s,
     pj_r,
 ):
     n_z = n_tp // CORES
@@ -185,42 +171,70 @@
             src_ref=src, dst_ref=dst, send_sem=send, recv_sem=recv, device_id=device, device_id_type=MESH
         )
 
-    def send(src, dst, send_sem, recv_sem, device):
-        copy = remote(src, dst, send_sem, recv_sem, device)
+    free = list(range(pool.shape[0]))
+
+    def send_done(entry):
+        entry[0].wait_send()
+        free.append(entry[1])
+        pending[:] = [one for one in pending if one is not entry]
+
+    def send(src, dst, recv_sem, device):
+        if not free:
+            send_done(pending[0])
+        index = free.pop(0)
+        copy = remote(src, dst, pool.at[index], recv_sem, device)
         copy.start()
-        pending.append(copy)
-        return copy
+        entry = (copy, index)
+        pending.append(entry)
+        return entry
 
     def arrived(view, sem):
         remote(view, view, sem, sem, partner).wait_recv()
 
-    def local(src, dst, index):
-        copy = pltpu.make_async_copy(src, dst, ld.at[index])
+    def local(src, dst):
+        index = free.pop(0)
+        copy = pltpu.make_async_copy(src, dst, pool.at[index])
         copy.start()
-        return copy
+        return copy, index
+
+    def here(*entries):
+        for copy, index in entries:
+            copy.wait()
+            free.append(index)
+
+    barrier = pltpu.get_barrier_semaphore()
+    peers = 0
+    for k in range(1, n_ep):
+        pl.semaphore_signal(barrier, inc=1, device_id=((e + k) % n_ep, t), device_id_type=MESH)
+        peers += 1
+    for k in range(1, n_z):
+        pl.semaphore_signal(barrier, inc=1, device_id=z_device(k), device_id_type=MESH)
+        peers += 1
+    pl.semaphore_signal(barrier, inc=1, device_id=partner, device_id_type=MESH)
+    peers += 1
 
     get_tok = [
-        local(tok_hbm.at[rows], rows_tok.at[e, rows], i)
+        local(tok_hbm.at[rows], rows_tok.at[e, rows])
         for i, rows in enumerate(
             pl.ds(pl.multiple_of(core * (tok_hbm.shape[0] // CORES), 32), tok_hbm.shape[0] // CORES)
             for core in (c, 1 - c)
         )
     ]
-    get_pnorm = local(pnorm_hbm, pnorm, 19 + n_ep)
-    get_eg = local(eg_hbm, eg, 20 + n_ep)
-    get_eu = local(eu_hbm, eu, 2)
-    get_ed = local(ed_hbm, ed, 3)
+    get_pnorm = local(pnorm_hbm, pnorm)
+    get_eg = local(eg_hbm, eg)
+    get_eu = local(eu_hbm, eu)
+    get_ed = local(ed_hbm, ed)
     lane_b = pl.ds(pl.multiple_of(pair * LANES, LANES), LANES)
-    get_x = local(x_hbm, xpad.at[pl.ds(HALO, length)], 4)
-    get_b = local(b_hbm.at[:, lane_b], bcpad.at[pl.ds(HALO, length), pl.ds(0, LANES)], 5)
-    get_c = local(c_hbm.at[:, lane_b], bcpad.at[pl.ds(HALO, length), pl.ds(LANES, LANES)], 6)
-    get_gate = local(gate_hbm, gate, 7)
+    get_x = local(x_hbm, xpad.at[pl.ds(HALO, length)])
+    get_b = local(b_hbm.at[:, lane_b], bcpad.at[pl.ds(HALO, length), pl.ds(0, LANES)])
+    get_c = local(c_hbm.at[:, lane_b], bcpad.at[pl.ds(HALO, length), pl.ds(LANES, LANES)])
+    get_gate = local(gate_hbm, gate)
     get_w = [
-        local(wout_hbm.at[:, pl.ds(q * part, part)], wk.at[q, z], 8 + q) for q in range(n_ep)
+        local(wout_hbm.at[:, pl.ds(q * part, part)], wk.at[q, z]) for q in range(n_ep)
     ]
 
     get_small = [
-        local(src, dst, 8 + n_ep + i)
+        local(src, dst)
         for i, (src, dst) in enumerate(
             (
                 (grouter_hbm, grouter),
@@ -238,19 +252,8 @@
         )
     ]
 
-    barrier = pltpu.get_barrier_semaphore()
-    peers = 0
-    for k in range(1, n_ep):
-        pl.semaphore_signal(barrier, inc=1, device_id=((e + k) % n_ep, t), device_id_type=MESH)
-        peers += 1
-    for k in range(1, n_z):
-        pl.semaphore_signal(barrier, inc=1, device_id=z_device(k), device_id_type=MESH)
-        peers += 1
-    pl.semaphore_signal(barrier, inc=1, device_id=partner, device_id_type=MESH)
-    peers += 1
-
-    get_pnorm.wait()
-    get_tok[0].wait()
+    here(get_pnorm)
+    here(get_tok[0])
     scale = pnorm[...].astype(F32).reshape(1, depth)
 
     def norm_rows(i, carry):
@@ -270,16 +273,15 @@
         if piece == 0:
             first, count = core * half + way * quarter, quarter
         else:
-            count = quarter // 2
-            first = core * half + (1 - way) * quarter + (piece - 1) * count
+            first, count = core * half + (1 - way) * quarter, quarter
         return rows_tok.at[block, pl.ds(pl.multiple_of(first, count), count), :]
 
     def pieces_of(d):
-        return range(1 if d == half_ring else 3)
+        return range(1 if d == half_ring else 2)
 
     def send_tokens(way, d, piece):
         view = tok_view(c, way, d - 1, piece)
-        send(view, view, tok_s.at[way, d - 1, piece], tok_r.at[way, d - 1, piece], toward[way])
+        send(view, view, tok_r.at[way, d - 1, piece], toward[way])
 
     def share_tokens(d, pieces):
         for piece in pieces:
@@ -288,7 +290,7 @@
                 arrived(view, tok_r.at[way, d - 1, piece])
                 if d < half_ring and piece in pieces_of(d + 1):
                     send_tokens(way, d + 1, piece)
-                send(view, view, tokp_s.at[way, d - 1, piece], tokp_r.at[way, d - 1, piece], partner)
+                send(view, view, tokp_r.at[way, d - 1, piece], partner)
 
     def shared_tokens(way, d):
         for piece in pieces_of(d):
@@ -325,14 +327,13 @@
     z_order = sorted(range(1, n_z), key=lambda k: (k != 1, -k))
 
     def weight_along_z(k):
-        send(wout_hbm.at[:, mine], wk.at[e, z], wz_s.at[k - 1], wz_r.at[k - 1], z_device(k))
+        send(wout_hbm.at[:, mine], wk.at[e, z], wz_r.at[k - 1], z_device(k))
 
     for k in z_order[:-1]:
         weight_along_z(k)
 
-    get_tok[1].wait()
-    for copy in get_small:
-        copy.wait()
+    here(get_tok[1])
+    here(*get_small)
     lax.fori_loop((1 - c) * steps, (1 - c) * steps + steps, norm_rows, 0)
 
     for way in range(2):
@@ -374,7 +375,7 @@
             picks[1] == i, share[1], 0.0
         )
     for k in range(1, n_ep):
-        send(wts.at[e], wts.at[e], wts_s.at[k - 1], wts_r.at[k - 1], ((e + k) % n_ep, t))
+        send(wts.at[e], wts.at[e], wts_r.at[k - 1], ((e + k) % n_ep, t))
 
     slots = psend.shape[0]
     to_partner = {}
@@ -396,8 +397,8 @@
         slot = order % slots
         if order >= slots:
             earlier = to_partner[order - slots]
-            earlier.wait_send()
-            pending[:] = [copy for copy in pending if copy is not earlier]
+            if any(one is earlier for one in pending):
+                send_done(earlier)
 
         def down(into, core):
             for k in range(n_z):
@@ -407,7 +408,7 @@
 
         down(psend.at[slot], 1 - c)
         to_partner[order] = send(
-            psend.at[slot], precv.at[block], pd_s.at[order], pd_r.at[order], partner
+            psend.at[slot], precv.at[block], pd_r.at[order], partner
         )
         down(pmine.at[block], c)
 
@@ -441,9 +442,9 @@
             pieces.append(jnp.where(lane < STATE, low, high))
         return jnp.concatenate(pieces, axis=1) if len(pieces) > 1 else pieces[0]
 
-    get_x.wait()
-    get_b.wait()
-    get_c.wait()
+    here(get_x)
+    here(get_b)
+    here(get_c)
 
     @pl.when(e > 0)
     def _():
@@ -484,6 +485,13 @@
 
     lax.fori_loop(0, nblk, first_pass, 0)
 
+    def order_of(way, d):
+        if d == half_ring:
+            return 2 * d - 1
+        if d == 0:
+            return 0
+        return 2 * d - 1 + way
+
     half_w = rows_w // 2
 
     def weight_view(block, way, k, d):
@@ -498,7 +506,7 @@
     def send_weight(way, d, k):
         if on_ring(d, k):
             view = weight_view(at_ring(-(d - 1) if way == 0 else d - 1), way, k, d)
-            send(view, view, wr_s.at[way, d - 1, k - 1], wr_r.at[way, d - 1, k - 1], toward[way])
+            send(view, view, wr_r.at[way, d - 1, k - 1], toward[way])
 
     def first_weight(k):
         arrived(wk.at[e, across_z(k)], wz_r.at[k - 1])
@@ -518,15 +526,24 @@
     def direct_rows(d):
         return pl.ds(0, rows_w) if d == half_ring else pl.ds(half_w, rows_w - half_w)
 
-    def direct_weight(block, order, d):
-        cols = pl.ds(pl.multiple_of(block * part, part), part)
-        send(
-            wout_hbm.at[direct_rows(d), cols],
-            wk.at[block, z, direct_rows(d), :],
-            wx_s.at[order - 1],
-            wx_r.at[order - 1],
-            z_device(1),
-        )
+    def direct_weights():
+        entries = []
+        targets = [(way, d) for d in range(1, half_ring) for way in range(2)] + [(0, half_ring)]
+        for way, d in targets:
+            block = at_ring(-d if way == 0 else d)
+            cols = pl.ds(pl.multiple_of(block * part, part), part)
+            index = free.pop(0)
+            copy = remote(
+                wout_hbm.at[direct_rows(d), cols],
+                wk.at[block, z, direct_rows(d), :],
+                pool.at[index],
+                wx_r.at[order_of(way, d) - 1],
+                z_device(1),
+            )
+            entries.append((copy, index))
+        return entries
+
+    two_sided = (z > 0) & (z < n_z - 1)
 
     def direct_arrived(block, order, d):
         arrived(wk.at[block, across_z(1), direct_rows(d), :], wx_r.at[order - 1])
@@ -540,20 +557,20 @@
     ]
     for k, copy in enumerate(state_copies):
         pl.when(e + 1 + k < n_ep)(copy.start)
-    get_eg.wait()
-    get_eu.wait()
-    get_ed.wait()
+    here(get_eg)
+    here(get_eu)
+    here(get_ed)
     weight_along_z(z_order[-1])
+    direct = direct_weights()
+
+    @pl.when(two_sided)
+    def _():
+        for copy, _index in direct:
+            copy.start()
+
     share_tokens(1, [0])
     experts(e, 0)
     share_tokens(1, [1])
-
-    def order_of(way, d):
-        if d == half_ring:
-            return 2 * d - 1
-        if d == 0:
-            return 0
-        return 2 * d - 1 + way
 
     def partner_sum(block, order):
         arrived(precv.at[block], pd_r.at[order])
@@ -569,7 +586,7 @@
             pmine[block, :, cols] = value.astype(BF16)
             view = pmine.at[block, :, cols]
             send(
-                view, rsrecv.at[way, d - 1, :, cols], rs_s.at[way, d - 1], rs_r.at[way, d - 1], toward[way]
+                view, rsrecv.at[way, d - 1, :, cols], rs_r.at[way, d - 1], toward[way]
             )
             return
         last = d == half_ring - 1
@@ -584,10 +601,10 @@
             ).astype(BF16)
             if d == 1:
                 view = rsrecv.at[way, 0, :, at]
-                send(pmine.at[block, :, at], view, rsl_s.at[way, k], rsl_r.at[way, k], toward[way])
+                send(pmine.at[block, :, at], view, rsl_r.at[way, k], toward[way])
         if d > 1:
             send(
-                pmine.at[block], rsrecv.at[way, d - 1], rs_s.at[way, d - 1], rs_r.at[way, d - 1], toward[way]
+                pmine.at[block], rsrecv.at[way, d - 1], rs_r.at[way, d - 1], toward[way]
             )
 
     def chunk_of(k):
@@ -603,7 +620,7 @@
             gone = srecv[k, STATE : STATE + 16, :].astype(F32)[0:1, :]
             ent[group_rows, :] = before * gone + srecv[k, 0:STATE, :].astype(F32)
 
-    get_gate.wait()
+    here(get_gate)
     head_lane = lax.broadcasted_iota(jnp.int32, (1, width), 1) // STATE
     d_row = jnp.zeros((1, width), F32)
     for h in range(heads):
@@ -657,7 +674,7 @@
         lax.fori_loop(0, per_chip, body, 0)
         view = mixed.at[pl.ds(pl.multiple_of(target * chip_rows, chip_rows), chip_rows), :]
         if k:
-            send(view, mrecv.at[z], a2a_s.at[k - 1], a2a_r.at[k - 1], z_device(k))
+            send(view, mrecv.at[z], a2a_r.at[k - 1], z_device(k))
         else:
             own = pl.ds(pl.multiple_of(z * chip_rows, chip_rows), chip_rows)
             mrecv[z] = mixed[own, :]
@@ -670,13 +687,15 @@
     mixes = [k for k in range(2, n_z)] + [1, 0]
     waiting = list(z_order)
     mix_for(mixes.pop(0))
-    share_tokens(1, [2])
     first_weight(waiting.pop(0))
     first_weight(waiting.pop(0))
-    for d in range(1, half_ring):
-        for way in range(2):
-            direct_weight(at_ring(-d if way == 0 else d), order_of(way, d), d)
-    direct_weight(at_ring(half_ring), order_of(0, half_ring), half_ring)
+
+    @pl.when(jnp.logical_not(two_sided))
+    def _():
+        for copy, _index in direct:
+            copy.start()
+
+    pending.extend(direct)
     for k in range(1, n_ep):
         arrived(wts.at[(e - k + n_ep) % n_ep], wts_r.at[k - 1])
     for way in range(2):
@@ -718,13 +737,11 @@
     partner_sum(e, 0)
     for k in reversed(range(1, n_z)):
         zsend[k - 1] = own_sum(k).astype(BF16)
-        send(zsend.at[k - 1], zrecv.at[k - 1], zs_s.at[k - 1], zs_r.at[k - 1], z_device(k))
-    eown[...] = own_sum(0)
+        send(zsend.at[k - 1], zrecv.at[k - 1], zs_r.at[k - 1], z_device(k))
 
     for k in range(1, n_z):
         arrived(mrecv.at[across_z(k)], a2a_r.at[k - 1])
-    for copy in get_w:
-        copy.wait()
+    here(*get_w)
 
     def rows_of(core):
         return pl.ds(pl.multiple_of(core * rows_dev, rows_dev), rows_dev)
@@ -736,7 +753,7 @@
         return total
 
     def give(order):
-        send(pjsend.at[order], pjrecv.at[order], pj_s.at[order], pj_r.at[order], partner)
+        send(pjsend.at[order], pjrecv.at[order], pj_r.at[order], partner)
 
     def project(block, order):
         pjsend[order] = product(1 - c, block).astype(BF16)
@@ -762,18 +779,10 @@
                 for core, total in zip(both, (pjown.at[order], pjlast)):
                     total[...] += dot(mrecv[place, rows_of(core), :], wk[block, place])
 
-    puts = []
-
-    def put(src, dst, index):
-        copy = pltpu.make_async_copy(src, dst, ld.at[index])
-        copy.start()
-        puts.append(copy)
-
     def finish(block, order):
         arrived(pjrecv.at[order], pj_r.at[order])
-        result[order] = (pjown[order] + pjrecv[order].astype(F32)).astype(BF16)
         cols = pl.ds(pl.multiple_of(block * part, part), part)
-        put(result.at[order], out.at[:, cols], order)
+        out[:, cols] = (pjown[order] + pjrecv[order].astype(F32)).astype(BF16)
 
     project(e, 0)
     done = [(e, 0)]
@@ -784,22 +793,21 @@
             project(block, order_of(way, d))
             done.append((block, order_of(way, d)))
 
+    eown[...] = own_sum(0)
+    for block, order in done:
+        finish(block, order)
+    project_late(at_ring(half_ring), order_of(0, half_ring))
+
     total = eown[...]
     for k in range(1, n_z):
         arrived(zrecv.at[k - 1], zs_r.at[k - 1])
         total = total + zrecv[k - 1].astype(F32)
-    eresult[...] = total.astype(BF16)
-    put(eresult, eout, n_ep)
-
-    for block, order in done:
-        finish(block, order)
-    project_late(at_ring(half_ring), order_of(0, half_ring))
+    eout[...] = total.astype(BF16)
+
     finish(at_ring(half_ring), order_of(0, half_ring))
 
-    for copy in pending:
+    for copy, _ in pending:
         copy.wait_send()
-    for copy in puts:
-        copy.wait()
 
     @pl.when(e < n_ep - 1)
     def _():
@@ -810,35 +818,26 @@
         pl.when(e + 1 + k < n_ep)(copy.wait_send)
 
 
-def hand_over_kernel(chunks, a_in, b_in, a_out, b_out, a, b, sems):
-    rows = a.shape[0] // chunks
-    moves = [(a_in.at[pl.ds(i * rows, rows)], a.at[pl.ds(i * rows, rows)], a_out.at[pl.ds(i * rows, rows)]) for i in range(chunks)]
-    moves.append((b_in, b, b_out))
-    reads = [pltpu.make_async_copy(m[0], m[1], sems.at[0, i]) for i, m in enumerate(moves)]
-    writes = [pltpu.make_async_copy(m[1], m[2], sems.at[1, i]) for i, m in enumerate(moves)]
-    for copy in reads:
+def hand_over_kernel(a, b, a_out, b_out, sems):
+    copies = [
+        pltpu.make_async_copy(src, dst, sems.at[i])
+        for i, (src, dst) in enumerate(((a, a_out), (b, b_out)))
+    ]
+    for copy in copies:
         copy.start()
-    for read, write in zip(reads, writes):
-        read.wait()
-        write.start()
-    for copy in writes:
+    for copy in copies:
         copy.wait()
 
 
 def hand_over(a, b):
-    chunks = 8
-    anywhere = pl.BlockSpec(memory_space=pl.ANY)
     return pl.pallas_call(
-        functools.partial(hand_over_kernel, chunks),
+        hand_over_kernel,
         out_shape=(jax.ShapeDtypeStruct(a.shape, a.dtype), jax.ShapeDtypeStruct(b.shape, b.dtype)),
-        in_specs=[anywhere] * 2,
-        out_specs=(anywhere, anywhere),
-        scratch_shapes=[
-            pltpu.VMEM(a.shape, a.dtype),
-            pltpu.VMEM(b.shape, b.dtype),
-            pltpu.SemaphoreType.DMA((2, chunks + 1)),
-        ],
+        in_specs=[pl.BlockSpec(memory_space=pltpu.VMEM)] * 2,
+        out_specs=(pl.BlockSpec(memory_space=pl.ANY),) * 2,
+        scratch_shapes=[pltpu.SemaphoreType.DMA((2,))],
         name="hand_over",
+        compiler_params=pltpu.CompilerParams(vmem_limit_bytes=8_000_000),
     )(a, b)
 
 
@@ -905,6 +904,7 @@
     slots = max(2, min(n_ep, 16 // n_ep))
     keep = n_z * feats
     anywhere = pl.BlockSpec(memory_space=pl.ANY)
+    vmem = pl.BlockSpec(memory_space=pltpu.VMEM)
     dma = pltpu.SemaphoreType.DMA
     scratch = [
         (pltpu.SMEM if v.dtype == F32 and v.ndim == 1 else pltpu.VMEM)(v.shape, v.dtype)
@@ -943,20 +943,18 @@
         pltpu.VMEM((n_ep, rows_dev, part), F32),
         pltpu.VMEM((rows_dev, part), F32),
         pltpu.VMEM((n_ep, rows_dev, part), BF16),
-        pltpu.VMEM((n_ep, rows_dev, part), BF16),
-        pltpu.VMEM((n_tok, feats), BF16),
         pltpu.VMEM((n_tok, feats), F32),
-        dma((21 + n_ep,)),
+        dma((29 + 2 * n_ep,)),
         dma((3,)),
         dma((3,)),
     ]
+    scratch += [dma((n_ep - 1,)), dma((n_ep - 1,))]
     for shape in (
-        (2, half_ring, 3),
-        (2, half_ring, 3),
+        (2, half_ring, 2),
+        (2, half_ring, 2),
         (n_ep - 1,),
         (n_z - 1,),
         (2, half_ring, n_z - 1),
-        (n_ep - 1,),
         (n_ep - 1,),
         (n_ep,),
         (2, half_ring),
@@ -965,7 +963,8 @@
         (n_z - 1,),
         (n_ep,),
     ):
-        scratch += [dma(shape), dma(shape)]
+        scratch.append(dma(shape))
+    grant = 67_000_000 if n_ep > 4 else 48_000_000
     mixer_out, experts_out = pl.pallas_call(
         functools.partial(kernel, n_ep, n_tp),
         out_shape=(
@@ -973,13 +972,13 @@
             jax.ShapeDtypeStruct((n_tok, feats), BF16),
         ),
         in_specs=[anywhere] * len(operands),
-        out_specs=(anywhere, anywhere),
+        out_specs=(vmem, vmem),
         scratch_shapes=scratch,
         name="fused",
         compiler_params=pltpu.CompilerParams(
-            collective_id=0, has_side_effects=True, vmem_limit_bytes=67_000_000
+            collective_id=0, has_side_effects=True, vmem_limit_bytes=grant
         ),
-    )(*operands)
+    )(*[pltpu.with_memory_space_constraint(v, pltpu.HBM) for v in operands])
     return hand_over(mixer_out, experts_out)
 
 

time: 72.3 us -> 68 us (0.941)
  Pallas kernels: 71.1 us -> 67.1 us
    pallas_call x1, Pallas kernels: 68.9 us -> 66.1 us  [fused(): pl.pallas_call(functools.partial(kernel, n_ep, n_tp), out_shape=(jax.Shap...]
    pallas_call x1, Pallas kernels: 2.15 us -> 1.02 us  [hand_over(): pl.pallas_call(hand_over_kernel, out_shape=(jax.ShapeDtypeStruct(a.shape,...]
where the time goes in v4:
time: 68 us; the launch traced here: 67.9 us
  Pallas kernels  67.1 us (99%)
  between operations  0.81 us (1%)
    pallas_call x1, Pallas kernels, fused(): pl.pallas_call(functools.partial(kernel, n_ep, n_tp), out_shape=(jax.Shap...  66.1 us

profile of v4, /device:TPU:0, one launch (start us, length us, event | category | flops | bytes accessed | tf_op | source)
XLA Modules:
  0.0 67.9 jit_solution(11770551487772448550)
XLA Ops:
  0.6 66.1 %fused.1 = (bf16[256,2048]{1,0:T(8,128)(2,1)S(1)}, bf16[256,256]{1,0:T(8,128)(2,1)S(1)}) custom-call(bf16[2048,256]{1,0:T(8,128)(2,1)} %x_hbm.1, bf16[2048,256]{1,0:T(8,128)(2,1)} %gate_hbm.1, bf16[2048,256]{1,0:T(8,128)(2,1)} %b_hbm.1, bf16[2048,256]{1,0:T(8,128)(2,1)} %c_hbm.1, bf16[256,2048]{1,0:T(8,128)(2,1)} %wout_hbm.1, bf16[256,2048]{1,0:T(8,128)(2,1)} %tok_hbm.1, ...), custom_call_target="tpu_custom_call" | custom-call | tf_op jit(solution)/shard_map/fused/pallas_call | solution.py:968
  66.7 1.0 %hand_over.1 = (bf16[256,2048]{1,0:T(8,128)(2,1)}, bf16[256,256]{1,0:T(8,128)(2,1)}) custom-call(bf16[256,2048]{1,0:T(8,128)(2,1)S(1)} %get-tuple-element.4.a, bf16[256,256]{1,0:T(8,128)(2,1)S(1)} %get-tuple-element.5.b), custom_call_target="tpu_custom_call" | custom-call | tf_op jit(solution)/shard_map/hand_over/pallas_call | solution.py:833

commit v5 on v4

--- a/solution.py
+++ b/solution.py
@@ -492,13 +492,13 @@
             return 0
         return 2 * d - 1 + way
 
-    half_w = rows_w // 2
+    half_w, ring_w = rows_w // 2, rows_w // 2
 
     def weight_view(block, way, k, d):
         slab = wk.at[block, across_z(k)]
         if d == half_ring:
             return slab.at[pl.ds(way * half_w, half_w), :]
-        return slab.at[pl.ds(0, half_w), :] if k == 1 else slab
+        return slab.at[pl.ds(0, ring_w), :] if k == 1 else slab
 
     def on_ring(d, k):
         return k != 1 or d < half_ring
@@ -524,7 +524,7 @@
             send_weight(way, d + 1, k)
 
     def direct_rows(d):
-        return pl.ds(0, rows_w) if d == half_ring else pl.ds(half_w, rows_w - half_w)
+        return pl.ds(0, rows_w) if d == half_ring else pl.ds(ring_w, rows_w - ring_w)
 
     def direct_weights():
         entries = []
@@ -685,7 +685,7 @@
             ring_sum(d, way)
 
     mixes = [k for k in range(2, n_z)] + [1, 0]
-    waiting = list(z_order)
+    waiting = [z_order[1], z_order[0]] + z_order[2:]
     mix_for(mixes.pop(0))
     first_weight(waiting.pop(0))
     first_weight(waiting.pop(0))
@@ -708,6 +708,7 @@
         for way in range(2):
             shared_tokens(way, d + 1)
     experts(at_ring(half_ring), order_of(0, half_ring))
+    pass_weight(1, z_order[1])
     partner_sum(at_ring(half_ring), order_of(0, half_ring))
     for way in range(2):
         ring_sum(half_ring, way)
@@ -721,7 +722,8 @@
 
     for d in range(1, half_ring):
         for k in z_order:
-            pass_weight(d, k)
+            if (d, k) != (1, z_order[1]):
+                pass_weight(d, k)
 
     def own_sum(k):
         at = chunk_of(k)

time: 68 us -> 67.6 us (level)
  no operation moved by 1% of the time
where the time goes in v5:
time: 67.6 us; the launch traced here: 67.5 us
  Pallas kernels  66.7 us (99%)
  between operations  0.81 us (1%)
    pallas_call x1, Pallas kernels, fused(): pl.pallas_call(functools.partial(kernel, n_ep, n_tp), out_shape=(jax.Shap...  65.7 us

profile of v5, /device:TPU:0, one launch (start us, length us, event | category | flops | bytes accessed | tf_op | source)
XLA Modules:
  0.0 67.5 jit_solution(5995273215271797247)
XLA Ops:
  0.6 65.7 %fused.1 = (bf16[256,2048]{1,0:T(8,128)(2,1)S(1)}, bf16[256,256]{1,0:T(8,128)(2,1)S(1)}) custom-call(bf16[2048,256]{1,0:T(8,128)(2,1)} %x_hbm.1, bf16[2048,256]{1,0:T(8,128)(2,1)} %gate_hbm.1, bf16[2048,256]{1,0:T(8,128)(2,1)} %b_hbm.1, bf16[2048,256]{1,0:T(8,128)(2,1)} %c_hbm.1, bf16[256,2048]{1,0:T(8,128)(2,1)} %wout_hbm.1, bf16[256,2048]{1,0:T(8,128)(2,1)} %tok_hbm.1, ...), custom_call_target="tpu_custom_call" | custom-call | tf_op jit(solution)/shard_map/fused/pallas_call | solution.py:970
  66.3 1.0 %hand_over.1 = (bf16[256,2048]{1,0:T(8,128)(2,1)}, bf16[256,256]{1,0:T(8,128)(2,1)}) custom-call(bf16[256,2048]{1,0:T(8,128)(2,1)S(1)} %get-tuple-element.4.a, bf16[256,256]{1,0:T(8,128)(2,1)S(1)} %get-tuple-element.5.b), custom_call_target="tpu_custom_call" | custom-call | tf_op jit(solution)/shard_map/hand_over/pallas_call | solution.py:835
